TPU v7x, 32 devices: a whole 2x2x4 slice. The times are simulated.
32 devices in a mesh: grp: 2 (over y), sp: 4 (over z), tp: 4 (over x, core).
Axes of the slice: x: 2, y: 2, z: 4, core: 2. Of those that a mesh axis runs over, the one named last changes fastest.
Arguments:
- tokens: bfloat16 [2048, 2048], P(('grp', 'sp'), 'tp'), parts along dimension 0, may hold values from -6 to 6
- norm_gain: float32 [2048], replicated, may hold values from 0.1 to 1.9
- ret_query_weight: bfloat16 [2048, 256], P('sp', 'tp'), may hold values from -0.125 to 0.125
- ret_key_weight: bfloat16 [2048, 256], P('sp', 'tp'), may hold values from -0.125 to 0.125
- ret_value_weight: bfloat16 [2048, 512], P('sp', 'tp'), may hold values from -0.125 to 0.125
- fox_query_weight: bfloat16 [2048, 512], P('sp', 'tp'), may hold values from -8 to 8
- fox_key_weight: bfloat16 [2048, 512], P('sp', 'tp'), may hold values from -0.125 to 0.125
- fox_value_weight: bfloat16 [2048, 512], P('sp', 'tp'), may hold values from -0.125 to 0.125
- ret_decay: float32 [8], P('tp'), may hold values from -1 to 0, as said below
- ret_state: float32 [16, 32, 64], P(('grp', 'tp')), parts along dimension 0, may hold values from -64 to 64
- head_norm_gain: float32 [512], P('tp'), may hold values from 0.1 to 1.9
- fox_gates: float32 [2048, 8], P('grp', 'tp'), parts along dimension 0, may hold values from -3072 to 0, as said below
- ret_out_weight: bfloat16 [512, 2048], P('tp', 'sp'), may hold values from -0.1875 to 0.1875
- fox_out_weight: bfloat16 [512, 2048], P('tp', 'sp'), may hold values from -1 to 1
Outputs:
- mixed: bfloat16 [2048, 2048], P(('grp', 'sp', 'tp')), parts along dimension 0
There are 2 independent parts, one for each index of `grp`. A program takes and returns all parts, laid end to end along the dimension named above; an argument that names none is the same for every part. Nothing has to cross between parts.
Inputs may be any that keep to these rules, and one draw needn't show every extreme that they name: `ret_decay`: each head's log decay is negative. `fox_gates`: along the positions each head's column never rises.
All inputs are finite; a program needn't handle non-finite values.
Results may differ from a plain program's by a relative error of at most 0.015.
The roundings to bfloat16 on the way count: a program that leaves them out, or rounds other values in their place, can miss the bound.
Values may be sent and summed in bfloat16 or wider, within the bound.
A program may use at most 64 MiB of HBM per device.

v0:
```python
import functools

import jax
import jax.numpy as jnp
from jax import lax
from jax.experimental import pallas as pl
from jax.experimental.pallas import tpu as pltpu
from jax.sharding import PartitionSpec as P

epsilon = 1e-06
highest = lax.Precision.HIGHEST
NT = (((1,), (1,)), ((), ()))
TN = (((0,), (0,)), ((), ()))


def rdma(src, dst, send_sem, recv_sem, **target):
    return pltpu.make_async_remote_copy(
        src_ref=src,
        dst_ref=dst,
        send_sem=send_sem,
        recv_sem=recv_sem,
        device_id=target,
        device_id_type=pl.DeviceIdType.MESH,
    )


class LineGather:
    def __init__(self, owns, place, sems, n, n_grp, me, g):
        self.owns, self.place, self.n, self.n_grp, self.me, self.g = owns, place, n, n_grp, me, g
        self.up, self.down, self.zr, self.ys, self.yr, self.loc = sems
        self.arrays = len(owns)
        self.rows = owns[0].shape[0]
        self.step = self.rows // n_grp

    def piece(self, part, src, c):
        return self.place(src, c, part * self.step, self.step)

    def own_piece(self, c):
        return self.owns[c].at[pl.ds(pl.multiple_of(self.g * self.step, self.step), self.step)]

    def hop(self, sems, to, src, c, first=False):
        here = self.own_piece(c) if first else self.piece(self.g, src, c)
        at = src * self.arrays + c
        return rdma(here, self.piece(self.g, src, c), sems.at[at], self.zr.at[at], sp=to)

    def side(self, d, src, c):
        at = ((d - 1) * self.n + src) * self.arrays + c
        here = self.piece(self.g, src, c)
        return rdma(here, here, self.ys.at[at], self.yr.at[at], grp=lax.rem(self.g + d, self.n_grp))

    def side_in(self, d, src, c):
        at = ((d - 1) * self.n + src) * self.arrays + c
        part = lax.rem(self.g + self.n_grp - d, self.n_grp)
        here = self.piece(part, src, c)
        return rdma(here, here, self.ys.at[at], self.yr.at[at], grp=part)

    def local(self, c):
        return pltpu.make_async_copy(self.owns[c], self.place(self.me, c, 0, self.rows), self.loc.at[c])

    def start(self):
        me, n = self.me, self.n
        for c in range(self.arrays):

            @pl.when(me + 1 < n)
            def _():
                self.hop(self.up, me + 1, me, c, True).start()

            @pl.when(me >= 1)
            def _():
                self.hop(self.down, me - 1, me, c, True).start()

        for c in range(self.arrays):
            self.local(c).start()

    def relay(self, k):
        me, n = self.me, self.n
        for c in range(self.arrays):
            for src, sems, to in ((me - k, self.up, me + 1), (me + k, self.down, me - 1)):

                @pl.when((src >= 0) & (src < n))
                def _(src=src, sems=sems, to=to):
                    self.hop(sems, me, src, c).wait_recv()

                    @pl.when((to >= 0) & (to < n))
                    def _():
                        self.hop(sems, to, src, c).start()

                    for d in range(1, self.n_grp):
                        self.side(d, src, c).start()

    def arrive_shard(self, src, arrays):
        for c in arrays:
            for d in range(1, self.n_grp):
                self.side_in(d, src, c).wait_recv()

    def arrive(self, arrays):
        for c in arrays:
            self.local(c).wait()

        def step(k, _):
            self.arrive_shard(lax.rem(self.me + k, self.n), arrays)
            return 0

        lax.fori_loop(1, self.n, step, 0)

    def finish(self):
        me, n = self.me, self.n

        def step(src, _):
            for c in range(self.arrays):

                @pl.when((src <= me) & (me + 1 < n))
                def _():
                    self.hop(self.up, me, src, c).wait_send()

                @pl.when((src >= me) & (me >= 1))
                def _():
                    self.hop(self.down, me, src, c).wait_send()

                @pl.when(src != me)
                def _():
                    for d in range(1, self.n_grp):
                        self.side(d, src, c).wait_send()

            return 0

        lax.fori_loop(0, n, step, 0)


def kernel(
    size,
    tok_ref,
    gain_ref,
    wq_ref,
    wk_ref,
    wrv_ref,
    wfq_ref,
    wfk_ref,
    wfv_ref,
    decay_ref,
    state_ref,
    hgain_ref,
    gates_ref,
    ret_out_ref,
    fox_out_ref,
    out_ref,
    tok_buf,
    qk_own,
    w_buf,
    wout_buf,
    norm_buf,
    proj_buf,
    kv_buf,
    sum_buf,
    mix_buf,
    rs_send,
    pair_buf,
    pair_sum,
    rs_buf,
    top_buf,
    total_buf,
    weighted_buf,
    tok_s,
    tok_r,
    tok_loc,
    kv_s,
    kv_r,
    sum_s,
    sum_r,
    pair_s,
    pair_r,
    rs_s,
    rs_r,
    *gather_sems,
):
    n, n_tp, n_grp, hr, dk, vd, fh, fd, direct = size
    me, t, g = lax.axis_index("sp"), lax.axis_index("tp"), lax.axis_index("grp")
    rows, feats = tok_ref.shape
    owns = [wfk_ref, wfv_ref, wfq_ref, wrv_ref, qk_own]
    early = 2
    starts = [0]
    for own in owns:
        starts.append(starts[-1] + own.shape[1])
    shard = qk_own.shape[0]

    def weight_place(src, c, first, count):
        start = pl.multiple_of(src * shard + first, count)
        return w_buf.at[pl.ds(start, count), starts[c] : starts[c + 1]]

    depth = mix_buf.shape[1] // 2
    out_cols = ret_out_ref.shape[1] if direct else ret_out_ref.shape[0]

    def out_place(src, c, first, count):
        if direct:
            start = pl.multiple_of(c * depth + first, count)
            return wout_buf.at[pl.ds(start, count), pl.ds(pl.multiple_of(src * out_cols, out_cols), out_cols)]
        start = pl.multiple_of(src * out_cols + first, count)
        return wout_buf.at[pl.ds(start, count), c * depth : (c + 1) * depth]

    def late_place(src, c, first, count):
        return weight_place(src, c + early, first, count)

    firsts = LineGather(owns[:early], weight_place, gather_sems[:6], n, n_grp, me, g)
    lasts = LineGather(owns[early:], late_place, gather_sems[6:12], n, n_grp, me, g)
    outs = LineGather([ret_out_ref, fox_out_ref], out_place, gather_sems[12:], n, n_grp, me, g)

    barrier = pltpu.get_barrier_semaphore()

    def greet(**target):
        pl.semaphore_signal(barrier, inc=1, device_id=target, device_id_type=pl.DeviceIdType.MESH)

    has_up, has_down = me + 1 < n, me >= 1
    for d in range(1, n_tp):
        greet(tp=lax.rem(t + d, n_tp))
    for d in range(1, n_grp):
        greet(grp=lax.rem(g + d, n_grp))

    @pl.when(has_up)
    def _():
        greet(sp=me + 1)

    @pl.when(has_down)
    def _():
        greet(sp=me - 1)

    turned = jnp.concatenate((wq_ref[...], wk_ref[...]), axis=0).astype(jnp.float32)
    qk_own[...] = turned.T.astype(jnp.bfloat16)

    count = n_tp - 1 + n_grp - 1 + has_up.astype(jnp.int32) + has_down.astype(jnp.int32)
    pl.semaphore_wait(barrier, count)

    def tok_copy(d):
        return rdma(tok_ref, tok_buf.at[t], tok_s.at[d - 1], tok_r.at[d - 1], tp=lax.rem(t + d, n_tp))

    def tok_in(d):
        src = lax.rem(t + n_tp - d, n_tp)
        return rdma(tok_ref, tok_buf.at[src], tok_s.at[d - 1], tok_r.at[d - 1], tp=src)

    firsts.start()
    lasts.start()
    tok_local = pltpu.make_async_copy(tok_ref, tok_buf.at[t], tok_loc)
    for d in range(1, n_tp):
        tok_copy(d).start()
    tok_local.start()

    def first_step(k, _):
        firsts.relay(k)

        lasts.relay(k)
        return 0

    lax.fori_loop(1, n, first_step, 0)
    outs.start()

    tok_local.wait()
    for d in range(1, n_tp):
        tok_in(d).wait_recv()
    squares = jnp.zeros((rows, 1), jnp.float32)
    for i in range(n_tp):
        part = tok_buf[i].astype(jnp.float32)
        squares = squares + jnp.sum(part * part, axis=-1, keepdims=True)
    scale = lax.rsqrt(squares * (1.0 / (n_tp * feats)) + epsilon)
    for i in range(n_tp):
        part = tok_buf[i].astype(jnp.float32)
        cols = slice(i * feats, (i + 1) * feats)
        norm_buf[:, cols] = (part * scale * gain_ref[:, cols]).astype(jnp.bfloat16)

    def kv_copy(src):
        return rdma(kv_buf.at[src], kv_buf.at[src], kv_s.at[src], kv_r.at[src], sp=jnp.minimum(me + 1, n - 1))

    def sum_copy(src):
        return rdma(sum_buf.at[src], sum_buf.at[src], sum_s.at[src], sum_r.at[src], sp=jnp.minimum(me + 1, n - 1))

    firsts.arrive((0, 1))
    kv_buf[me] = jnp.dot(
        norm_buf[...], w_buf[:, : starts[2]], preferred_element_type=jnp.float32
    ).astype(jnp.bfloat16)

    def kv_forward(k):
        src = me - k

        @pl.when(src >= 0)
        def _():
            kv_copy(src).wait_recv()

            @pl.when(has_up)
            def _():
                kv_copy(src).start()

    @pl.when(has_up)
    def _():
        kv_copy(me).start()

    outs.relay(1)
    lasts.arrive((0, 1, 2))
    proj_buf[...] = jnp.dot(
        norm_buf[...], w_buf[:, starts[2] :], preferred_element_type=jnp.float32
    ).astype(jnp.bfloat16)
    rv_at, rq_at = starts[3] - starts[2], starts[4] - starts[2]

    key_scale = dk ** (-0.5)
    position = lax.broadcasted_iota(jnp.int32, (rows, 1), 0).astype(jnp.float32)
    rq, rk, rv = [], [], []
    for h in range(hr):
        rq.append(proj_buf[:, rq_at + h * dk : rq_at + (h + 1) * dk])
        rk.append(proj_buf[:, rq_at + (hr + h) * dk : rq_at + (hr + h + 1) * dk])
        rv.append(proj_buf[:, rv_at + h * vd : rv_at + (h + 1) * vd])
        keys = rk[h].astype(jnp.float32) * key_scale
        trailing = jnp.exp((rows - 1.0 - position) * decay_ref[h])
        sum_buf[me, h] = lax.dot_general(
            keys * trailing, rv[h].astype(jnp.float32), TN, precision=highest, preferred_element_type=jnp.float32
        )

    @pl.when(has_up)
    def _():
        sum_copy(me).start()

    row_id = lax.broadcasted_iota(jnp.int32, (rows, rows), 0)
    col_id = lax.broadcasted_iota(jnp.int32, (rows, rows), 1)
    causal = col_id <= row_id
    own_cols = pl.ds(pl.multiple_of(me * rows, rows), rows)
    own_gates = [
        jnp.sum(jnp.where(row_id == col_id, gates_ref[h : h + 1, own_cols], 0.0), axis=1, keepdims=True)
        for h in range(fh)
    ]

    def attend(src, diagonal):
        key_cols = pl.ds(pl.multiple_of(src * rows, rows), rows)
        for h in range(fh):
            query = proj_buf[:, h * fd : (h + 1) * fd]
            k = kv_buf[src, :, h * fd : (h + 1) * fd]
            v = kv_buf[src, :, (fh + h) * fd : (fh + h + 1) * fd]
            logits = lax.dot_general(query, k, NT, preferred_element_type=jnp.float32) * fd ** (-0.5)
            logits = logits + own_gates[h] - gates_ref[h : h + 1, key_cols]
            if diagonal:
                logits = jnp.where(causal, logits, -jnp.inf)
            top_new = jnp.max(logits, axis=-1, keepdims=True)
            if not diagonal:
                top = top_buf[h]
                top_new = jnp.maximum(top, top_new)
            p = jnp.exp(logits - top_new)
            total = jnp.sum(p, axis=-1, keepdims=True)
            weighted = jnp.dot(p.astype(jnp.bfloat16), v, preferred_element_type=jnp.float32)
            if not diagonal:
                rescale = jnp.exp(top - top_new)
                total = total_buf[h] * rescale + total
                weighted = weighted_buf[h] * rescale + weighted
            top_buf[h] = top_new
            total_buf[h] = total
            weighted_buf[h] = weighted

    def forward(k):
        src = me - k

        @pl.when(src >= 0)
        def _():
            sum_copy(src).wait_recv()

            @pl.when(has_up)
            def _():
                sum_copy(src).start()

    attend(me, True)

    offset = (me * rows).astype(jnp.float32)
    lone = jnp.zeros((dk, vd), jnp.float32)

    def step(k, entering):
        src = me - k
        kv_forward(k)
        forward(k)

        @pl.when(k + 1 < n)
        def _():
            outs.relay(k + 1)


        @pl.when(src >= 0)
        def _():
            attend(src, False)

        gap = ((k - 1) * rows).astype(jnp.float32)
        there = jnp.maximum(src, 0)
        return tuple(
            entering[h]
            + jnp.where(src >= 0, jnp.exp(lone + gap * decay_ref[h]) * sum_buf[there, h], 0.0)
            for h in range(hr)
        )

    entering = tuple(jnp.exp(lone + offset * decay_ref[h]) * state_ref[h] for h in range(hr))
    entering = lax.fori_loop(1, n, step, entering)

    distance = jnp.maximum(row_id - col_id, 0).astype(jnp.float32)
    for h in range(hr):
        scores = lax.dot_general(rq[h], rk[h], NT, preferred_element_type=jnp.float32) * key_scale
        scores = jnp.where(causal, scores * jnp.exp(distance * decay_ref[h]), 0.0)
        inner = jnp.dot(scores, rv[h].astype(jnp.float32), precision=highest, preferred_element_type=jnp.float32)
        leading = jnp.exp((position + 1.0) * decay_ref[h])
        carried = jnp.dot(
            rq[h].astype(jnp.float32), entering[h], precision=highest, preferred_element_type=jnp.float32
        )
        raw = inner + carried * leading
        center = raw - jnp.mean(raw, axis=-1, keepdims=True)
        variance = jnp.mean(center * center, axis=-1, keepdims=True)
        cols = slice(h * vd, (h + 1) * vd)
        mix_buf[:, cols] = (center * lax.rsqrt(variance + epsilon) * hgain_ref[:, cols]).astype(jnp.bfloat16)
    for h in range(fh):
        cols = slice(hr * vd + h * fd, hr * vd + (h + 1) * fd)
        mix_buf[:, cols] = (weighted_buf[h] / total_buf[h]).astype(jnp.bfloat16)

    block = rows // n_tp
    columns = pair_buf.shape[1]
    wide = out_cols if direct else columns
    pieces = columns // wide
    half = n_tp // 2
    parity, pair = lax.rem(t, 2), lax.div(t, 2)

    def piece_cols(piece):
        return pl.ds(pl.multiple_of(piece * wide, wide), wide)

    def slot(at):
        return pl.ds(pl.multiple_of(at * block, block), block)

    def pair_copy(piece):
        cols = piece_cols(piece)
        return rdma(
            rs_send.at[1 - parity, :, cols],
            pair_buf.at[:, cols],
            pair_s.at[piece],
            pair_r.at[piece],
            tp=t + 1 - 2 * parity,
        )

    def rs_copy(d, piece):
        to = lax.rem(pair + d, half)
        cols = piece_cols(piece)
        at = (d - 1) * pieces + piece
        return rdma(
            pair_sum.at[slot(to), cols], rs_buf.at[d - 1, :, cols], rs_s.at[at], rs_r.at[at], tp=2 * to + parity
        )

    def project(piece):
        cols = piece_cols(piece)
        if direct:
            value = jnp.dot(mix_buf[...], wout_buf[:, cols], preferred_element_type=jnp.float32)
        else:
            value = lax.dot_general(mix_buf[...], wout_buf[...], NT, preferred_element_type=jnp.float32)
        value = value.astype(jnp.bfloat16)
        for b in range(n_tp):
            at = slice(b // 2 * block, (b // 2 + 1) * block)
            rs_send[b % 2, at, cols] = value[b * block : (b + 1) * block]
        pair_copy(piece).start()

    def reduce(piece):
        cols = piece_cols(piece)
        pair_copy(piece).wait_recv()
        both = rs_send[parity, :, cols].astype(jnp.float32) + pair_buf[:, cols].astype(jnp.float32)
        pair_sum[:, cols] = both.astype(jnp.bfloat16)
        for d in range(1, half):
            rs_copy(d, piece).start()

    def order(i):
        falling = jnp.where(i <= me, me - i, i)
        rising = jnp.where(i <= n - 1 - me, me + i, n - 1 - i)
        return jnp.where(2 * me >= n, falling, rising)

    if direct:
        for c in range(2):
            outs.local(c).wait()
        project(me)

        def out_step(i, _):
            outs.arrive_shard(order(i), (0, 1))
            project(order(i))
            reduce(order(i - 1))
            return 0

        lax.fori_loop(1, n, out_step, 0)
        reduce(order(jnp.int32(n - 1)))
    else:
        outs.arrive((0, 1))
        project(0)
        reduce(0)

    own = slot(pair)
    summed = rs_send[parity, own, :].astype(jnp.float32) + pair_buf[own, :].astype(jnp.float32)
    for d in range(1, half):
        for piece in range(pieces):
            rs_copy(d, piece).wait_recv()
        summed = summed + rs_buf[d - 1].astype(jnp.float32)
    out_ref[...] = summed.astype(jnp.bfloat16)

    for d in range(1, n_tp):
        tok_copy(d).wait_send()
    for piece in range(pieces):
        pair_copy(piece).wait_send()
        for d in range(1, half):
            rs_copy(d, piece).wait_send()
    firsts.finish()
    lasts.finish()
    outs.finish()

    @pl.when(has_up)
    def _():
        def step(src, _):
            kv_copy(src).wait_send()
            sum_copy(src).wait_send()
            return 0

        lax.fori_loop(0, me + 1, step, 0)


def local(
    n,
    n_tp,
    n_grp,
    tokens,
    norm_gain,
    ret_query_weight,
    ret_key_weight,
    ret_value_weight,
    fox_query_weight,
    fox_key_weight,
    fox_value_weight,
    ret_decay,
    ret_state,
    head_norm_gain,
    fox_gates,
    ret_out_weight,
    fox_out_weight,
):
    rows, feats = tokens.shape
    hr, dk, vd = ret_state.shape
    fh = fox_gates.shape[1]
    fd = fox_query_weight.shape[1] // fh
    shard = ret_query_weight.shape[0]
    width = 2 * hr * dk + hr * vd + 3 * fh * fd
    depth, out_cols = ret_out_weight.shape
    columns = out_cols * n
    direct = out_cols % 128 == 0
    if not direct:
        ret_out_weight, fox_out_weight = ret_out_weight.T, fox_out_weight.T
    dma = pltpu.SemaphoreType.DMA

    def gather_sems(arrays):
        side = max(n_grp - 1, 1) * n * arrays
        return [
            dma((n * arrays,)),
            dma((n * arrays,)),
            dma((n * arrays,)),
            dma((side,)),
            dma((side,)),
            dma((arrays,)),
        ]

    vmem = pl.BlockSpec(memory_space=pltpu.VMEM)
    smem = pl.BlockSpec(memory_space=pltpu.SMEM)
    hbm = pl.BlockSpec(memory_space=pl.ANY)
    size = (n, n_tp, n_grp, hr, dk, vd, fh, fd, direct)
    block = rows // n_tp
    peers = max(n_tp - 1, 1)
    far = max(n_tp // 2 - 1, 1)
    pieces = n if direct else 1
    return pl.pallas_call(
        functools.partial(kernel, size),
        out_shape=jax.ShapeDtypeStruct((block, columns), jnp.bfloat16),
        in_specs=[hbm, vmem, vmem, vmem, hbm, hbm, hbm, hbm, smem, vmem, vmem, vmem, hbm, hbm],
        out_specs=vmem,
        scratch_shapes=[
            pltpu.VMEM((n_tp, rows, feats), jnp.bfloat16),
            pltpu.VMEM((shard, 2 * hr * dk), jnp.bfloat16),
            pltpu.VMEM((n * shard, width), jnp.bfloat16),
            pltpu.VMEM((2 * depth, columns) if direct else (columns, 2 * depth), jnp.bfloat16),
            pltpu.VMEM((rows, n_tp * feats), jnp.bfloat16),
            pltpu.VMEM((rows, width - 2 * fh * fd), jnp.bfloat16),
            pltpu.VMEM((n, rows, 2 * fh * fd), jnp.bfloat16),
            pltpu.VMEM((n, hr, dk, vd), jnp.float32),
            pltpu.VMEM((rows, 2 * depth), jnp.bfloat16),
            pltpu.VMEM((2, rows // 2, columns), jnp.bfloat16),
            pltpu.VMEM((rows // 2, columns), jnp.bfloat16),
            pltpu.VMEM((rows // 2, columns), jnp.bfloat16),
            pltpu.VMEM((far, block, columns), jnp.bfloat16),
            pltpu.VMEM((fh, rows, 1), jnp.float32),
            pltpu.VMEM((fh, rows, 1), jnp.float32),
            pltpu.VMEM((fh, rows, fd), jnp.float32),
            dma((peers,)),
            dma((peers,)),
            dma,
            dma((n,)),
            dma((n,)),
            dma((n,)),
            dma((n,)),
            dma((pieces,)),
            dma((pieces,)),
            dma((far * pieces,)),
            dma((far * pieces,)),
        ]
        + gather_sems(2)
        + gather_sems(3)
        + gather_sems(2),
        compiler_params=pltpu.CompilerParams(
            collective_id=0, has_side_effects=True, vmem_limit_bytes=56 * 1024 * 1024
        ),
        name="layer",
    )(
        tokens,
        norm_gain[None, :],
        ret_query_weight.T,
        ret_key_weight.T,
        ret_value_weight,
        fox_query_weight,
        fox_key_weight,
        fox_value_weight,
        ret_decay,
        ret_state,
        head_norm_gain[None, :],
        fox_gates.T,
        ret_out_weight,
        fox_out_weight,
    )


def solution(mesh):
    placed = (
        P(("grp", "sp"), "tp"),
        P(),
        P("sp", "tp"),
        P("sp", "tp"),
        P("sp", "tp"),
        P("sp", "tp"),
        P("sp", "tp"),
        P("sp", "tp"),
        P("tp"),
        P(("grp", "tp"), None, None),
        P("tp"),
        P("grp", "tp"),
        P("tp", "sp"),
        P("tp", "sp"),
    )
    body = functools.partial(local, mesh.shape["sp"], mesh.shape["tp"], mesh.shape["grp"])
    return jax.shard_map(
        body, mesh=mesh, in_specs=placed, out_specs=P(("grp", "sp", "tp"), None), check_vma=False
    )
```

profile of v0, /device:TPU:25, one launch (start us, length us, event | category | flops | bytes accessed | tf_op | source)
XLA Modules:
  0.0 59.6 jit_solution(13496924155989551722)
XLA Ops:
  0.0 57.9 %layer.1 = bf16[64,2048]{1,0:T(8,128)(2,1)} custom-call(bf16[256,512]{1,0:T(8,128)(2,1)} %tok_ref.1, f32[1,2048]{1,0:T(1,128)} %bitcast.7, bf16[64,512]{1,0:T(8,128)(2,1)} %bitcast.5, bf16[64,512]{1,0:T(8,128)(2,1)} %bitcast.6, bf16[512,128]{1,0:T(8,128)(2,1)} %wrv_ref.1, bf16[512,128]{1,0:T(8,128)(2,1)} %wfq_ref.1, bf16[512,128]{1,0:T(8,128)(2,1)} %wfk_ref.1, ...), custom_call_target="tpu_custom_call" | custom-call | tf_op jit(solution)/shard_map/layer/pallas_call | solution.py:564
  57.9 1.7 %copy.16 = bf16[64,2048]{1,0:T(8,128)(2,1)} copy(bf16[64,2048]{1,0:T(8,128)(2,1)} %layer.1) | data formatting | bytes 524288
where the time goes:
time: 59.8 us; the launch traced here: 59.6 us
  Pallas kernels  57.9 us (97%)
  local copies, waits for them, and re-layouts  1.67 us (3%)
    pallas_call x1, Pallas kernels, local(): pl.pallas_call(functools.partial(kernel, size), out_shape=jax.ShapeDtypeS...  57.9 us
    unnamed x1, local copies, waits for them, and re-layouts  1.67 us

commit v1 on v0

--- a/solution.py
+++ b/solution.py
@@ -510,6 +510,748 @@
         lax.fori_loop(0, me + 1, step, 0)
 
 
+def pair_kernel(
+    size,
+    tok_ref,
+    gain_ref,
+    wq_ref,
+    wk_ref,
+    wrv_ref,
+    wfq_ref,
+    wfk_ref,
+    wfv_ref,
+    decay_ref,
+    state_ref,
+    hgain_ref,
+    gates_ref,
+    ret_out_ref,
+    fox_out_ref,
+    out_ref,
+    tok_buf,
+    qk_own,
+    w_buf,
+    wout_buf,
+    norm_buf,
+    proj_buf,
+    kv_buf,
+    sum_buf,
+    mix_pair,
+    mix_buf,
+    rs_send,
+    pair_buf,
+    pair_sum,
+    rs_buf,
+    top_buf,
+    total_buf,
+    weighted_buf,
+    tz_s,
+    tz_r,
+    tx_s,
+    tx_r,
+    tc_s,
+    tc_r,
+    t_loc,
+    w_s,
+    w_r,
+    wy_s,
+    wy_r,
+    w_loc,
+    kv_s,
+    kv_r,
+    sum_s,
+    sum_r,
+    mix_s,
+    mix_r,
+    pair_s,
+    pair_r,
+    rs_s,
+    rs_r,
+    *out_sems,
+):
+    n, n_tp, n_grp, hr, dk, vd, fh, fd, chunks = size
+    me, t, g = lax.axis_index("sp"), lax.axis_index("tp"), lax.axis_index("grp")
+    rows, feats = tok_ref.shape
+    shard = qk_own.shape[0]
+    couples = n // 2
+    couple, mine = lax.div(me, 2), lax.rem(me, 2)
+    other = 1 - mine
+    partner = me + 1 - 2 * mine
+    fox_mine = 1 - lax.rem(couple, 2)
+    is_fox = mine == fox_mine
+    is_ret = mine != fox_mine
+    lower = 2 * me < n
+    half = n_tp // 2
+    parity, pair = lax.rem(t, 2), lax.div(t, 2)
+
+    def fox_of(q):
+        return 2 * q + 1 - lax.rem(q, 2)
+
+    def ret_of(q):
+        return 2 * q + lax.rem(q, 2)
+
+    def toward(k):
+        return lax.rem(jnp.where(lower, me + k, me + n - k), n)
+
+    barrier = pltpu.get_barrier_semaphore()
+
+    def greet(**target):
+        pl.semaphore_signal(barrier, inc=1, device_id=target, device_id_type=pl.DeviceIdType.MESH)
+
+    greet(tp=2 * pair + 1 - parity)
+    for d in range(1, half):
+        greet(tp=2 * lax.rem(pair + d, half) + parity)
+    for d in range(1, n_grp):
+        greet(grp=lax.rem(g + d, n_grp))
+    for k in range(1, n):
+        greet(sp=lax.rem(me + k, n))
+
+    turned = jnp.concatenate((wq_ref[...], wk_ref[...]), axis=0).astype(jnp.float32)
+    qk_own[...] = turned.T.astype(jnp.bfloat16)
+
+    pl.semaphore_wait(barrier, half + n_grp - 1 + n - 1)
+
+    slab = rows // chunks
+
+    def own_tok(m):
+        return tok_ref.at[pl.ds(m * slab, slab)]
+
+    def tok_at(h, m, src):
+        return tok_buf.at[h, src, pl.ds(m * slab, slab)]
+
+    def tok_z(m):
+        return rdma(own_tok(m), tok_at(mine, m, t), tz_s.at[m], tz_r.at[m], sp=partner)
+
+    def tok_z_in(m):
+        here = tok_at(other, m, t)
+        return rdma(here, here, tz_s.at[m], tz_r.at[m], sp=partner)
+
+    def x_sem(own, m, d):
+        return ((0 if own else 1) * chunks + m) * max(half - 1, 1) + d - 1
+
+    def tok_x(own, m, d):
+        at = x_sem(own, m, d)
+        h = mine if own else other
+        src = own_tok(m) if own else tok_at(h, m, t)
+        return rdma(src, tok_at(h, m, t), tx_s.at[at], tx_r.at[at], tp=2 * lax.rem(pair + d, half) + parity)
+
+    def tok_x_in(own, m, d):
+        at = x_sem(own, m, d)
+        src = 2 * lax.rem(pair + half - d, half) + parity
+        here = tok_at(mine if own else other, m, src)
+        return rdma(here, here, tx_s.at[at], tx_r.at[at], tp=src)
+
+    def c_sem(own, m, d):
+        return ((0 if own else 1) * chunks + m) * half + d
+
+    def tok_c(own, m, d):
+        at = c_sem(own, m, d)
+        h = mine if own else other
+        src = 2 * lax.rem(pair + half - d, half) + parity
+        there = tok_at(h, m, src)
+        here = own_tok(m) if own and d == 0 else there
+        return rdma(here, there, tc_s.at[at], tc_r.at[at], tp=2 * pair + 1 - parity)
+
+    def tok_c_in(own, m, d):
+        at = c_sem(own, m, d)
+        src = 2 * lax.rem(pair + half - d, half) + 1 - parity
+        here = tok_at(mine if own else other, m, src)
+        return rdma(here, here, tc_s.at[at], tc_r.at[at], tp=2 * pair + 1 - parity)
+
+    tok_local = pltpu.make_async_copy(tok_ref, tok_buf.at[mine, t], t_loc)
+
+    for m in range(chunks):
+        tok_z(m).start()
+        for d in range(1, half):
+            tok_x(True, m, d).start()
+        tok_c(True, m, 0).start()
+
+    owns = [wfk_ref, wfv_ref, wfq_ref, wrv_ref, qk_own]
+    fox_arrays, ret_arrays = (0, 1, 2), (3, 4)
+    starts = {}
+    for group in (fox_arrays, ret_arrays):
+        at = 0
+        for c in group:
+            starts[c] = (at, at + owns[c].shape[1])
+            at = starts[c][1]
+    fox_wide, ret_wide = starts[2][1], starts[4][1]
+    q_at = starts[2][0]
+    step = shard // n_grp
+    count = len(owns)
+
+    def w_at(c, src, part):
+        start = pl.multiple_of(src * shard + part * step, step)
+        return w_buf.at[pl.ds(start, step), starts[c][0] : starts[c][1]]
+
+    def w_send(c, to):
+        here = owns[c].at[pl.ds(pl.multiple_of(g * step, step), step)]
+        return rdma(here, w_at(c, me, g), w_s.at[to * count + c], w_r.at[me * count + c], sp=to)
+
+    def w_in(c, src):
+        here = w_at(c, src, g)
+        return rdma(here, here, w_s.at[src * count + c], w_r.at[src * count + c], sp=src)
+
+    def w_side(c, src, d):
+        at = ((d - 1) * n + src) * count + c
+        here = w_at(c, src, g)
+        return rdma(here, here, wy_s.at[at], wy_r.at[at], grp=lax.rem(g + d, n_grp))
+
+    def w_side_in(c, src, d):
+        at = ((d - 1) * n + src) * count + c
+        part = lax.rem(g + n_grp - d, n_grp)
+        here = w_at(c, src, part)
+        return rdma(here, here, wy_s.at[at], wy_r.at[at], grp=part)
+
+    def w_local(c):
+        start = pl.multiple_of(me * shard, shard)
+        return pltpu.make_async_copy(
+            owns[c], w_buf.at[pl.ds(start, shard), starts[c][0] : starts[c][1]], w_loc.at[c]
+        )
+
+    def each_target(arrays, whose, act):
+        for c in arrays:
+            for i in range(couples):
+                to = whose(jnp.where(lower, i, couples - 1 - i))
+
+                @pl.when(to != me)
+                def _(c=c, to=to):
+                    act(w_send(c, to))
+
+    def send_weights(act):
+        each_target((0, 1), fox_of, act)
+        each_target((2,), fox_of, act)
+        each_target(ret_arrays, ret_of, act)
+
+    send_weights(lambda copy: copy.start())
+    tok_local.start()
+
+    @pl.when(is_fox)
+    def _():
+        for c in fox_arrays:
+            w_local(c).start()
+
+    @pl.when(is_ret)
+    def _():
+        for c in ret_arrays:
+            w_local(c).start()
+
+    depth = mix_buf.shape[1] // 2
+    out_cols = ret_out_ref.shape[1]
+
+    def out_place(src, c, first, rows_):
+        start = pl.multiple_of(c * depth + first, rows_)
+        return wout_buf.at[pl.ds(start, rows_), pl.ds(pl.multiple_of(src * out_cols, out_cols), out_cols)]
+
+    outs = LineGather([ret_out_ref, fox_out_ref], out_place, out_sems, n, n_grp, me, g)
+    outs.start()
+
+    def w_relay(arrays, ks):
+        for k in ks:
+            for c in arrays:
+                w_in(c, toward(k)).wait_recv()
+                for d in range(1, n_grp):
+                    w_side(c, toward(k), d).start()
+
+    def w_arrive(arrays):
+        for c in arrays:
+            w_local(c).wait()
+            for k in range(1, n):
+                for d in range(1, n_grp):
+                    w_side_in(c, toward(k), d).wait_recv()
+
+    def normalize(h):
+        squares = jnp.zeros((rows, 1), jnp.float32)
+        for i in range(n_tp):
+            part = tok_buf[h, i].astype(jnp.float32)
+            squares = squares + jnp.sum(part * part, axis=-1, keepdims=True)
+        scale = lax.rsqrt(squares * (1.0 / (n_tp * feats)) + epsilon)
+        at = pl.ds(pl.multiple_of(h * rows, rows), rows)
+        for i in range(n_tp):
+            part = tok_buf[h, i].astype(jnp.float32)
+            cols = slice(i * feats, (i + 1) * feats)
+            norm_buf[at, cols] = (part * scale * gain_ref[:, cols]).astype(jnp.bfloat16)
+
+    far = list(range(2, n - 1))
+
+    @pl.when(is_fox)
+    def _():
+        w_relay(fox_arrays, [1])
+
+    for m in range(chunks):
+        for d in range(1, half):
+            tok_x_in(True, m, d).wait_recv()
+            tok_c(True, m, d).start()
+        tok_z_in(m).wait_recv()
+        for d in range(1, half):
+            tok_x(False, m, d).start()
+        tok_c(False, m, 0).start()
+
+    @pl.when(is_fox)
+    def _():
+        w_relay((0, 1), [n - 1])
+
+    @pl.when(is_ret)
+    def _():
+        w_relay(ret_arrays, [1])
+
+    tok_local.wait()
+    for m in range(chunks):
+        for d in range(half):
+            tok_c_in(True, m, d).wait_recv()
+    normalize(mine)
+
+    for m in range(chunks):
+        for d in range(1, half):
+            tok_x_in(False, m, d).wait_recv()
+            tok_c(False, m, d).start()
+
+    @pl.when(is_fox)
+    def _():
+        w_relay((0, 1), far)
+
+    @pl.when(is_ret)
+    def _():
+        w_relay(ret_arrays, far)
+
+    for m in range(chunks):
+        for d in range(half):
+            tok_c_in(False, m, d).wait_recv()
+    normalize(other)
+    outs.relay(1)
+
+    row_id = lax.broadcasted_iota(jnp.int32, (rows, rows), 0)
+    col_id = lax.broadcasted_iota(jnp.int32, (rows, rows), 1)
+    causal = col_id <= row_id
+
+    def norm_rows(h):
+        return norm_buf[pl.ds(pl.multiple_of(h * rows, rows), rows), :]
+
+    def mix_copy(first):
+        return rdma(
+            mix_pair.at[other], mix_buf.at[:, first : first + depth], mix_s.at[0], mix_r.at[0], sp=partner
+        )
+
+    def mix_own(first):
+        mix_buf[:, first : first + depth] = mix_pair[mine]
+
+    def mix_in(first):
+        here = mix_buf.at[:, first : first + depth]
+        return rdma(here, here, mix_s.at[0], mix_r.at[0], sp=partner)
+
+    def kv_copy(b, q):
+        at = 2 * couple + b
+        return rdma(kv_buf.at[at], kv_buf.at[at], kv_s.at[2 * q + b], kv_r.at[at], sp=fox_of(q))
+
+    def kv_in(at):
+        return rdma(kv_buf.at[at], kv_buf.at[at], kv_s.at[at], kv_r.at[at], sp=partner)
+
+    def sum_copy(q):
+        return rdma(sum_buf.at[couple], sum_buf.at[couple], sum_s.at[q], sum_r.at[couple], sp=ret_of(q))
+
+    def sum_in(q):
+        return rdma(sum_buf.at[q], sum_buf.at[q], sum_s.at[q], sum_r.at[q], sp=partner)
+
+    def later(act):
+        for q in range(1, couples):
+
+            @pl.when(q > couple)
+            def _(q=q):
+                act(jnp.int32(q))
+
+    @pl.when(is_fox)
+    def _():
+        w_arrive((0, 1))
+
+        def kv_step(i, _):
+            b = jnp.where(i == 0, mine, other)
+            kv_buf[2 * couple + b] = jnp.dot(
+                norm_rows(b), w_buf[:, :q_at], preferred_element_type=jnp.float32
+            ).astype(jnp.bfloat16)
+            later(lambda q: kv_copy(b, q).start())
+            return 0
+
+        lax.fori_loop(0, 2, kv_step, 0)
+        w_relay((2,), [n - 1] + far)
+        w_arrive((2,))
+        proj_buf[:, : fh * fd] = jnp.dot(
+            norm_buf[...], w_buf[:, q_at:fox_wide], preferred_element_type=jnp.float32
+        ).astype(jnp.bfloat16)
+
+        def block_cols(at):
+            return pl.ds(pl.multiple_of(at * rows, rows), rows)
+
+        def attend(b, at, first):
+            q_rows = pl.ds(pl.multiple_of(b * rows, rows), rows)
+            for h in range(fh):
+                query = proj_buf[q_rows, h * fd : (h + 1) * fd]
+                k = kv_buf[at, :, h * fd : (h + 1) * fd]
+                v = kv_buf[at, :, (fh + h) * fd : (fh + h + 1) * fd]
+                own = jnp.sum(
+                    jnp.where(row_id == col_id, gates_ref[h : h + 1, block_cols(2 * couple + b)], 0.0),
+                    axis=1,
+                    keepdims=True,
+                )
+                logits = lax.dot_general(query, k, NT, preferred_element_type=jnp.float32) * fd ** (-0.5)
+                logits = logits + own - gates_ref[h : h + 1, block_cols(at)]
+                if first:
+                    logits = jnp.where(causal, logits, -jnp.inf)
+                top_new = jnp.max(logits, axis=-1, keepdims=True)
+                if not first:
+                    top = top_buf[b, h]
+                    top_new = jnp.maximum(top, top_new)
+                p = jnp.exp(logits - top_new)
+                total = jnp.sum(p, axis=-1, keepdims=True)
+                weighted = jnp.dot(p.astype(jnp.bfloat16), v, preferred_element_type=jnp.float32)
+                if not first:
+                    rescale = jnp.exp(top - top_new)
+                    total = total_buf[b, h] * rescale + total
+                    weighted = weighted_buf[b, h] * rescale + weighted
+                top_buf[b, h] = top_new
+                total_buf[b, h] = total
+                weighted_buf[b, h] = weighted
+
+        def settle(b):
+            for h in range(fh):
+                mix_pair[b, :, h * fd : (h + 1) * fd] = (weighted_buf[b, h] / total_buf[b, h]).astype(jnp.bfloat16)
+
+        def diagonal(b, _):
+            attend(b, 2 * couple + b, True)
+            return 0
+
+        lax.fori_loop(0, 2, diagonal, 0)
+        attend(1, 2 * couple, False)
+
+        @pl.when(couple == 0)
+        def _():
+            settle(other)
+            mix_copy(depth).start()
+
+        outs.relay(2)
+
+        def past(i, _):
+            q = lax.div(i, 2)
+            b = jnp.where(lax.rem(i, 2) == 0, fox_of(q) - 2 * q, 1 - (fox_of(q) - 2 * q))
+            at = 2 * q + b
+            kv_in(at).wait_recv()
+
+            def both(j, _):
+                row_half = jnp.where(j == 0, other, mine)
+                attend(row_half, at, False)
+
+                @pl.when((j == 0) & (i == 2 * couple - 1))
+                def _():
+                    settle(other)
+                    mix_copy(depth).start()
+
+                return 0
+
+            lax.fori_loop(0, 2, both, 0)
+            return 0
+
+        lax.fori_loop(0, 2 * couple, past, 0)
+        settle(mine)
+        mix_own(depth)
+        for k in range(3, n):
+            outs.relay(k)
+        mix_in(0).wait_recv()
+        mix_copy(depth).wait_send()
+        later(lambda q: kv_copy(0, q).wait_send())
+        later(lambda q: kv_copy(1, q).wait_send())
+
+    @pl.when(is_ret)
+    def _():
+        w_relay(ret_arrays, [n - 1])
+        w_arrive(ret_arrays)
+        proj_buf[:, :ret_wide] = jnp.dot(
+            norm_buf[...], w_buf[:, :ret_wide], preferred_element_type=jnp.float32
+        ).astype(jnp.bfloat16)
+        rv_at, rq_at = starts[3][0], starts[4][0]
+        key_scale = dk ** (-0.5)
+        position = lax.broadcasted_iota(jnp.int32, (rows, 1), 0).astype(jnp.float32)
+        distance = jnp.maximum(row_id - col_id, 0).astype(jnp.float32)
+        lone = jnp.zeros((dk, vd), jnp.float32)
+
+        def part(b, first, wide):
+            return proj_buf[pl.ds(pl.multiple_of(b * rows, rows), rows), first : first + wide]
+
+        def summary(b, h):
+            keys = part(b, rq_at + (hr + h) * dk, dk).astype(jnp.float32) * key_scale
+            trailing = jnp.exp((rows - 1.0 - position) * decay_ref[h])
+            return lax.dot_general(
+                keys * trailing,
+                part(b, rv_at + h * vd, vd).astype(jnp.float32),
+                TN,
+                precision=highest,
+                preferred_element_type=jnp.float32,
+            )
+
+        early = [summary(0, h) for h in range(hr)]
+        for h in range(hr):
+            sum_buf[couple, h] = jnp.exp(lone + float(rows) * decay_ref[h]) * early[h] + summary(1, h)
+        later(lambda q: sum_copy(q).start())
+        outs.relay(2)
+
+        offset = (couple * 2 * rows).astype(jnp.float32)
+
+        def gather(q, entering):
+            sum_in(q).wait_recv()
+            gap = ((couple - 1 - q) * 2 * rows).astype(jnp.float32)
+            return tuple(entering[h] + jnp.exp(lone + gap * decay_ref[h]) * sum_buf[q, h] for h in range(hr))
+
+        entering = tuple(jnp.exp(lone + offset * decay_ref[h]) * state_ref[h] for h in range(hr))
+        entering = lax.fori_loop(0, couple, gather, entering)
+        second = tuple(jnp.exp(lone + float(rows) * decay_ref[h]) * entering[h] + early[h] for h in range(hr))
+
+        def block(i, _):
+            b = jnp.where(i == 0, other, mine)
+            for h in range(hr):
+                rq = part(b, rq_at + h * dk, dk)
+                rk = part(b, rq_at + (hr + h) * dk, dk)
+                rv = part(b, rv_at + h * vd, vd)
+                scores = lax.dot_general(rq, rk, NT, preferred_element_type=jnp.float32) * key_scale
+                scores = jnp.where(causal, scores * jnp.exp(distance * decay_ref[h]), 0.0)
+                inner = jnp.dot(
+                    scores, rv.astype(jnp.float32), precision=highest, preferred_element_type=jnp.float32
+                )
+                leading = jnp.exp((position + 1.0) * decay_ref[h])
+                carried = jnp.dot(
+                    rq.astype(jnp.float32),
+                    jnp.where(b == 0, entering[h], second[h]),
+                    precision=highest,
+                    preferred_element_type=jnp.float32,
+                )
+                raw = inner + carried * leading
+                center = raw - jnp.mean(raw, axis=-1, keepdims=True)
+                variance = jnp.mean(center * center, axis=-1, keepdims=True)
+                cols = slice(h * vd, (h + 1) * vd)
+                mix_pair[b, :, cols] = (center * lax.rsqrt(variance + epsilon) * hgain_ref[:, cols]).astype(
+                    jnp.bfloat16
+                )
+
+            @pl.when(i == 0)
+            def _():
+                mix_copy(0).start()
+
+            return 0
+
+        lax.fori_loop(0, 2, block, 0)
+        mix_own(0)
+        for k in range(3, n):
+            outs.relay(k)
+        mix_in(depth).wait_recv()
+        mix_copy(0).wait_send()
+        later(lambda q: sum_copy(q).wait_send())
+
+    block = rows // n_tp
+    wide, pieces = out_cols, n
+
+    def piece_cols(piece):
+        return pl.ds(pl.multiple_of(piece * wide, wide), wide)
+
+    def slot(at):
+        return pl.ds(pl.multiple_of(at * block, block), block)
+
+    def pair_copy(piece):
+        cols = piece_cols(piece)
+        return rdma(
+            rs_send.at[1 - parity, :, cols],
+            pair_buf.at[:, cols],
+            pair_s.at[piece],
+            pair_r.at[piece],
+            tp=t + 1 - 2 * parity,
+        )
+
+    def rs_copy(d, piece):
+        to = lax.rem(pair + d, half)
+        cols = piece_cols(piece)
+        at = (d - 1) * pieces + piece
+        return rdma(
+            pair_sum.at[slot(to), cols], rs_buf.at[d - 1, :, cols], rs_s.at[at], rs_r.at[at], tp=2 * to + parity
+        )
+
+    def project(piece):
+        cols = piece_cols(piece)
+        value = jnp.dot(mix_buf[...], wout_buf[:, cols], preferred_element_type=jnp.float32).astype(jnp.bfloat16)
+        for b in range(n_tp):
+            at = slice(b // 2 * block, (b // 2 + 1) * block)
+            rs_send[b % 2, at, cols] = value[b * block : (b + 1) * block]
+        pair_copy(piece).start()
+
+    def reduce(piece):
+        cols = piece_cols(piece)
+        pair_copy(piece).wait_recv()
+        both = rs_send[parity, :, cols].astype(jnp.float32) + pair_buf[:, cols].astype(jnp.float32)
+        pair_sum[:, cols] = both.astype(jnp.bfloat16)
+        for d in range(1, half):
+            rs_copy(d, piece).start()
+
+    def order(i):
+        falling = jnp.where(i <= me, me - i, i)
+        rising = jnp.where(i <= n - 1 - me, me + i, n - 1 - i)
+        return jnp.where(lower, rising, falling)
+
+    for c in range(2):
+        outs.local(c).wait()
+    project(me)
+
+    def out_step(i, _):
+        outs.arrive_shard(order(i), (0, 1))
+        project(order(i))
+        reduce(order(i - 1))
+        return 0
+
+    lax.fori_loop(1, n, out_step, 0)
+    reduce(order(jnp.int32(n - 1)))
+
+    own = slot(pair)
+    summed = rs_send[parity, own, :].astype(jnp.float32) + pair_buf[own, :].astype(jnp.float32)
+    for d in range(1, half):
+        for piece in range(pieces):
+            rs_copy(d, piece).wait_recv()
+        summed = summed + rs_buf[d - 1].astype(jnp.float32)
+    out_ref[...] = summed.astype(jnp.bfloat16)
+
+    for m in range(chunks):
+        tok_z(m).wait_send()
+        for own_half in (True, False):
+            for d in range(1, half):
+                tok_x(own_half, m, d).wait_send()
+            for d in range(half):
+                tok_c(own_half, m, d).wait_send()
+    send_weights(lambda copy: copy.wait_send())
+
+    def sides(arrays):
+        for c in arrays:
+            for k in range(1, n):
+                for d in range(1, n_grp):
+                    w_side(c, toward(k), d).wait_send()
+
+    @pl.when(is_fox)
+    def _():
+        sides(fox_arrays)
+
+    @pl.when(is_ret)
+    def _():
+        sides(ret_arrays)
+
+    for piece in range(pieces):
+        pair_copy(piece).wait_send()
+        for d in range(1, half):
+            rs_copy(d, piece).wait_send()
+    outs.finish()
+
+
+def paired(n, n_tp, n_grp, inputs):
+    tokens, ret_query_weight, ret_state, fox_gates = inputs[0], inputs[2], inputs[9], inputs[11]
+    fox_query_weight, ret_out_weight = inputs[5], inputs[12]
+    rows, feats = tokens.shape
+    hr, dk, vd = ret_state.shape
+    fh = fox_gates.shape[1]
+    fd = fox_query_weight.shape[1] // fh
+    shard = ret_query_weight.shape[0]
+    depth, out_cols = ret_out_weight.shape
+    columns = out_cols * n
+    wide = max(3 * fh * fd, 2 * hr * dk + hr * vd)
+    half = n_tp // 2
+    block = rows // n_tp
+    chunks = 2
+    count = 5
+    couples = n // 2
+    dma = pltpu.SemaphoreType.DMA
+    far = max(half - 1, 1)
+    side = max(n_grp - 1, 1) * n
+    vmem = pl.BlockSpec(memory_space=pltpu.VMEM)
+    smem = pl.BlockSpec(memory_space=pltpu.SMEM)
+    hbm = pl.BlockSpec(memory_space=pl.ANY)
+    bf16, f32 = jnp.bfloat16, jnp.float32
+    size = (n, n_tp, n_grp, hr, dk, vd, fh, fd, chunks)
+    return pl.pallas_call(
+        functools.partial(pair_kernel, size),
+        out_shape=jax.ShapeDtypeStruct((block, columns), bf16),
+        in_specs=[hbm, vmem, vmem, vmem, hbm, hbm, hbm, hbm, smem, vmem, vmem, vmem, hbm, hbm],
+        out_specs=vmem,
+        scratch_shapes=[
+            pltpu.VMEM((2, n_tp, rows, feats), bf16),
+            pltpu.VMEM((shard, 2 * hr * dk), bf16),
+            pltpu.VMEM((n * shard, wide), bf16),
+            pltpu.VMEM((2 * depth, columns), bf16),
+            pltpu.VMEM((2 * rows, n_tp * feats), bf16),
+            pltpu.VMEM((2 * rows, wide), bf16),
+            pltpu.VMEM((n, rows, 2 * fh * fd), bf16),
+            pltpu.VMEM((couples, hr, dk, vd), f32),
+            pltpu.VMEM((2, rows, depth), bf16),
+            pltpu.VMEM((rows, 2 * depth), bf16),
+            pltpu.VMEM((2, rows // 2, columns), bf16),
+            pltpu.VMEM((rows // 2, columns), bf16),
+            pltpu.VMEM((rows // 2, columns), bf16),
+            pltpu.VMEM((far, block, columns), bf16),
+            pltpu.VMEM((2, fh, rows, 1), f32),
+            pltpu.VMEM((2, fh, rows, 1), f32),
+            pltpu.VMEM((2, fh, rows, fd), f32),
+            dma((chunks,)),
+            dma((chunks,)),
+            dma((2 * chunks * far,)),
+            dma((2 * chunks * far,)),
+            dma((2 * chunks * half,)),
+            dma((2 * chunks * half,)),
+            dma,
+            dma((n * count,)),
+            dma((n * count,)),
+            dma((side * count,)),
+            dma((side * count,)),
+            dma((count,)),
+            dma((2 * couples,)),
+            dma((n,)),
+            dma((couples,)),
+            dma((couples,)),
+            dma((1,)),
+            dma((1,)),
+            dma((n,)),
+            dma((n,)),
+            dma((far * n,)),
+            dma((far * n,)),
+            dma((n * 2,)),
+            dma((n * 2,)),
+            dma((n * 2,)),
+            dma((side * 2,)),
+            dma((side * 2,)),
+            dma((2,)),
+        ],
+        compiler_params=pltpu.CompilerParams(
+            collective_id=0, has_side_effects=True, vmem_limit_bytes=56 * 1024 * 1024
+        ),
+        name="layer",
+    )(
+        tokens,
+        inputs[1][None, :],
+        inputs[2].T,
+        inputs[3].T,
+        inputs[4],
+        inputs[5],
+        inputs[6],
+        inputs[7],
+        inputs[8],
+        inputs[9],
+        inputs[10][None, :],
+        inputs[11].T,
+        inputs[12],
+        inputs[13],
+    )
+
+
+def pairs_fit(n, n_tp, n_grp, inputs):
+    rows, feats = inputs[0].shape
+    hr, dk, vd = inputs[9].shape
+    shard = inputs[2].shape[0]
+    depth, out_cols = inputs[12].shape
+    wide = inputs[5].shape[1]
+    lanes = all(w % 128 == 0 for w in (out_cols, wide, 2 * hr * dk, hr * vd, feats, depth))
+    even = n % 2 == 0 and n > 2 and n_tp % 2 == 0
+    tiles = rows % (16 * n_tp) == 0 and rows % 32 == 0 and shard % (16 * n_grp) == 0 and depth % (16 * n_grp) == 0
+    columns = n * out_cols
+    held = 8 * rows * n_tp * feats + 2 * n * shard * 3 * wide + 4 * depth * columns + 4 * n * rows * wide + 6 * rows * columns
+    return lanes and even and tiles and depth == wide == hr * vd and held < 40 * 1024 * 1024
+
+
 def local(
     n,
     n_tp,
@@ -529,6 +1271,24 @@
     ret_out_weight,
     fox_out_weight,
 ):
+    inputs = (
+        tokens,
+        norm_gain,
+        ret_query_weight,
+        ret_key_weight,
+        ret_value_weight,
+        fox_query_weight,
+        fox_key_weight,
+        fox_value_weight,
+        ret_decay,
+        ret_state,
+        head_norm_gain,
+        fox_gates,
+        ret_out_weight,
+        fox_out_weight,
+    )
+    if pairs_fit(n, n_tp, n_grp, inputs):
+        return paired(n, n_tp, n_grp, inputs)
     rows, feats = tokens.shape
     hr, dk, vd = ret_state.shape
     fh = fox_gates.shape[1]

time: 59.8 us -> 57 us (0.953)
  the two profiles are of different devices: /device:TPU:25 before, /device:TPU:0 now
where the time goes in v1:
time: 57 us; the launch traced here: 56.8 us
  Pallas kernels  55.2 us (97%)
  local copies, waits for them, and re-layouts  1.67 us (3%)
    pallas_call x1, Pallas kernels, paired(): pl.pallas_call(functools.partial(pair_kernel, size), out_shape=jax.ShapeD...  55.2 us
    unnamed x1, local copies, waits for them, and re-layouts  1.67 us

profile of v1, /device:TPU:0, one launch (start us, length us, event | category | flops | bytes accessed | tf_op | source)
XLA Modules:
  0.0 56.8 jit_solution(17492105389239520473)
XLA Ops:
  0.0 55.2 %layer.1 = bf16[64,2048]{1,0:T(8,128)(2,1)} custom-call(bf16[256,512]{1,0:T(8,128)(2,1)} %tok_ref.1, f32[1,2048]{1,0:T(1,128)} %bitcast.7, bf16[64,512]{1,0:T(8,128)(2,1)} %bitcast.5, bf16[64,512]{1,0:T(8,128)(2,1)} %bitcast.6, bf16[512,128]{1,0:T(8,128)(2,1)} %wrv_ref.1, bf16[512,128]{1,0:T(8,128)(2,1)} %wfq_ref.1, bf16[512,128]{1,0:T(8,128)(2,1)} %wfk_ref.1, ...), custom_call_target="tpu_custom_call" | custom-call | tf_op jit(solution)/shard_map/layer/pallas_call | solution.py:1167
  55.2 1.7 %copy.16 = bf16[64,2048]{1,0:T(8,128)(2,1)} copy(bf16[64,2048]{1,0:T(8,128)(2,1)} %layer.1) | data formatting | bytes 524288

commit v2 on v1

--- a/solution.py
+++ b/solution.py
@@ -526,7 +526,15 @@
     gates_ref,
     ret_out_ref,
     fox_out_ref,
-    out_ref,
+    near_ref,
+    far_ref,
+    gain_buf,
+    wq_buf,
+    wk_buf,
+    state_buf,
+    hgain_buf,
+    gates_buf,
+    gate_col,
     tok_buf,
     qk_own,
     w_buf,
@@ -540,10 +548,14 @@
     rs_send,
     pair_buf,
     pair_sum,
-    rs_buf,
+    near_buf,
     top_buf,
     total_buf,
     weighted_buf,
+    in_sem,
+    near_sem,
+    above_sem,
+    below_sem,
     tz_s,
     tz_r,
     tx_s,
@@ -602,13 +614,67 @@
         greet(tp=2 * lax.rem(pair + d, half) + parity)
     for d in range(1, n_grp):
         greet(grp=lax.rem(g + d, n_grp))
-    for k in range(1, n):
-        greet(sp=lax.rem(me + k, n))
-
-    turned = jnp.concatenate((wq_ref[...], wk_ref[...]), axis=0).astype(jnp.float32)
+    has_up, has_down = me + 1 < n, me >= 1
+
+    @pl.when(has_up)
+    def _():
+        greet(sp=me + 1)
+
+    @pl.when(has_down)
+    def _():
+        greet(sp=me - 1)
+
+    brought = [
+        pltpu.make_async_copy(src, dst, in_sem.at[i])
+        for i, (src, dst) in enumerate(
+            (
+                (wq_ref, wq_buf),
+                (wk_ref, wk_buf),
+                (gain_ref, gain_buf),
+                (state_ref, state_buf),
+                (hgain_ref, hgain_buf),
+                (gates_ref, gates_buf),
+            )
+        )
+    ]
+    for copy in brought:
+        copy.start()
+    for copy in brought[:2]:
+        copy.wait()
+    turned = jnp.concatenate((wq_buf[...], wk_buf[...]), axis=0).astype(jnp.float32)
     qk_own[...] = turned.T.astype(jnp.bfloat16)
 
-    pl.semaphore_wait(barrier, half + n_grp - 1 + n - 1)
+    pl.semaphore_wait(barrier, half + n_grp - 1 + has_up.astype(jnp.int32) + has_down.astype(jnp.int32))
+
+    def tell(sem, to):
+        pl.semaphore_signal(sem, inc=1, device_id={"sp": to}, device_id_type=pl.DeviceIdType.MESH)
+
+    @pl.when(has_up & has_down)
+    def _():
+        tell(above_sem, me - 1)
+        tell(below_sem, me + 1)
+
+    def meet_far():
+        def from_above(i, _):
+            pl.semaphore_wait(above_sem, 1)
+
+            @pl.when(has_down)
+            def _():
+                tell(above_sem, me - 1)
+
+            return 0
+
+        def from_below(i, _):
+            pl.semaphore_wait(below_sem, 1)
+
+            @pl.when(has_up)
+            def _():
+                tell(below_sem, me + 1)
+
+            return 0
+
+        lax.fori_loop(0, jnp.maximum(n - 2 - me, 0), from_above, 0)
+        lax.fori_loop(0, jnp.maximum(me - 1, 0), from_below, 0)
 
     slab = rows // chunks
 
@@ -660,10 +726,8 @@
     tok_local = pltpu.make_async_copy(tok_ref, tok_buf.at[mine, t], t_loc)
 
     for m in range(chunks):
-        tok_z(m).start()
         for d in range(1, half):
             tok_x(True, m, d).start()
-        tok_c(True, m, 0).start()
 
     owns = [wfk_ref, wfv_ref, wfq_ref, wrv_ref, qk_own]
     fox_arrays, ret_arrays = (0, 1, 2), (3, 4)
@@ -682,9 +746,16 @@
         start = pl.multiple_of(src * shard + part * step, step)
         return w_buf.at[pl.ds(start, step), starts[c][0] : starts[c][1]]
 
-    def w_send(c, to):
+    def w_sem(c, src, up):
+        return ((0 if up else n) + src) * count + c
+
+    def w_send(c, to, up):
         here = owns[c].at[pl.ds(pl.multiple_of(g * step, step), step)]
-        return rdma(here, w_at(c, me, g), w_s.at[to * count + c], w_r.at[me * count + c], sp=to)
+        return rdma(here, w_at(c, me, g), w_s.at[w_sem(c, me, up)], w_r.at[me * count + c], sp=to)
+
+    def w_on(c, src, to, up):
+        here = w_at(c, src, g)
+        return rdma(here, here, w_s.at[w_sem(c, src, up)], w_r.at[src * count + c], sp=to)
 
     def w_in(c, src):
         here = w_at(c, src, g)
@@ -707,21 +778,31 @@
             owns[c], w_buf.at[pl.ds(start, shard), starts[c][0] : starts[c][1]], w_loc.at[c]
         )
 
-    def each_target(arrays, whose, act):
+    fox_up = jnp.where(is_ret & (mine == 0), partner, fox_of(couple + 1))
+    fox_down = jnp.where(is_ret & (mine == 1), partner, jnp.where(couple >= 1, fox_of(jnp.maximum(couple - 1, 0)), -1))
+    ret_up = jnp.where(is_fox & (mine == 0), partner, ret_of(couple + 1))
+    ret_down = jnp.where(is_fox & (mine == 1), partner, jnp.where(couple >= 1, ret_of(jnp.maximum(couple - 1, 0)), -1))
+
+    def send_weights(arrays, act):
+        up, down = (fox_up, fox_down) if arrays[0] in fox_arrays else (ret_up, ret_down)
         for c in arrays:
-            for i in range(couples):
-                to = whose(jnp.where(lower, i, couples - 1 - i))
-
-                @pl.when(to != me)
-                def _(c=c, to=to):
-                    act(w_send(c, to))
-
-    def send_weights(act):
-        each_target((0, 1), fox_of, act)
-        each_target((2,), fox_of, act)
-        each_target(ret_arrays, ret_of, act)
-
-    send_weights(lambda copy: copy.start())
+
+            @pl.when(up < n)
+            def _(c=c):
+                act(w_send(c, up, True))
+
+            @pl.when(down >= 0)
+            def _(c=c):
+                act(w_send(c, down, False))
+
+    def start(copy):
+        copy.start()
+
+    send_weights((0, 1), start)
+    for m in range(chunks):
+        tok_z(m).start()
+        tok_c(True, m, 0).start()
+    send_weights((2,), start)
     tok_local.start()
 
     @pl.when(is_fox)
@@ -742,12 +823,23 @@
         return wout_buf.at[pl.ds(start, rows_), pl.ds(pl.multiple_of(src * out_cols, out_cols), out_cols)]
 
     outs = LineGather([ret_out_ref, fox_out_ref], out_place, out_sems, n, n_grp, me, g)
-    outs.start()
+
+    def w_pass(c, src, act):
+        up, down = (fox_up, fox_down) if c in fox_arrays else (ret_up, ret_down)
+
+        @pl.when((src < me) & (up < n))
+        def _():
+            act(w_on(c, src, up, True))
+
+        @pl.when((src > me) & (down >= 0))
+        def _():
+            act(w_on(c, src, down, False))
 
     def w_relay(arrays, ks):
         for k in ks:
             for c in arrays:
                 w_in(c, toward(k)).wait_recv()
+                w_pass(c, toward(k), start)
                 for d in range(1, n_grp):
                     w_side(c, toward(k), d).start()
 
@@ -768,55 +860,55 @@
         for i in range(n_tp):
             part = tok_buf[h, i].astype(jnp.float32)
             cols = slice(i * feats, (i + 1) * feats)
-            norm_buf[at, cols] = (part * scale * gain_ref[:, cols]).astype(jnp.bfloat16)
+            norm_buf[at, cols] = (part * scale * gain_buf[:, cols]).astype(jnp.bfloat16)
 
     far = list(range(2, n - 1))
 
-    @pl.when(is_fox)
-    def _():
-        w_relay(fox_arrays, [1])
-
-    for m in range(chunks):
+    def tok_own(m):
         for d in range(1, half):
             tok_x_in(True, m, d).wait_recv()
             tok_c(True, m, d).start()
+
+    def tok_swap(m):
         tok_z_in(m).wait_recv()
         for d in range(1, half):
             tok_x(False, m, d).start()
         tok_c(False, m, 0).start()
 
-    @pl.when(is_fox)
-    def _():
-        w_relay((0, 1), [n - 1])
-
-    @pl.when(is_ret)
-    def _():
-        w_relay(ret_arrays, [1])
-
-    tok_local.wait()
-    for m in range(chunks):
-        for d in range(half):
-            tok_c_in(True, m, d).wait_recv()
-    normalize(mine)
-
-    for m in range(chunks):
+    def tok_last(m):
         for d in range(1, half):
             tok_x_in(False, m, d).wait_recv()
             tok_c(False, m, d).start()
 
+    def tok_ready(own):
+        if own:
+            tok_local.wait()
+        for m in range(chunks):
+            for d in range(half):
+                tok_c_in(own, m, d).wait_recv()
+
+    for copy in brought[2:]:
+        copy.wait()
+
+    @pl.when(is_fox)
+    def _():
+        w_relay((0, 1), [1, n - 1])
+
+    meet_far()
+    send_weights(ret_arrays, start)
+    outs.start()
+
+    for m in range(chunks):
+        tok_own(m)
+        tok_swap(m)
+
     @pl.when(is_fox)
     def _():
         w_relay((0, 1), far)
-
-    @pl.when(is_ret)
-    def _():
-        w_relay(ret_arrays, far)
-
-    for m in range(chunks):
-        for d in range(half):
-            tok_c_in(False, m, d).wait_recv()
-    normalize(other)
-    outs.relay(1)
+        w_relay((2,), [1])
+
+    tok_ready(True)
+    normalize(mine)
 
     row_id = lax.broadcasted_iota(jnp.int32, (rows, rows), 0)
     col_id = lax.broadcasted_iota(jnp.int32, (rows, rows), 1)
@@ -857,20 +949,26 @@
             def _(q=q):
                 act(jnp.int32(q))
 
+    def after_tokens():
+        for m in range(chunks):
+            tok_last(m)
+
     @pl.when(is_fox)
     def _():
-        w_arrive((0, 1))
-
-        def kv_step(i, _):
-            b = jnp.where(i == 0, mine, other)
+        def project_kv(b):
             kv_buf[2 * couple + b] = jnp.dot(
                 norm_rows(b), w_buf[:, :q_at], preferred_element_type=jnp.float32
             ).astype(jnp.bfloat16)
             later(lambda q: kv_copy(b, q).start())
-            return 0
-
-        lax.fori_loop(0, 2, kv_step, 0)
+
+        after_tokens()
+        w_arrive((0, 1))
+        project_kv(mine)
         w_relay((2,), [n - 1] + far)
+        tok_ready(False)
+        normalize(other)
+        project_kv(other)
+        outs.relay(1)
         w_arrive((2,))
         proj_buf[:, : fh * fd] = jnp.dot(
             norm_buf[...], w_buf[:, q_at:fox_wide], preferred_element_type=jnp.float32
@@ -878,6 +976,11 @@
 
         def block_cols(at):
             return pl.ds(pl.multiple_of(at * rows, rows), rows)
+
+        for b in range(2):
+            for h in range(fh):
+                own = jnp.where(row_id == col_id, gates_buf[h : h + 1, block_cols(2 * couple + b)], 0.0)
+                gate_col[b, h] = jnp.sum(own, axis=1, keepdims=True)
 
         def attend(b, at, first):
             q_rows = pl.ds(pl.multiple_of(b * rows, rows), rows)
@@ -885,13 +988,8 @@
                 query = proj_buf[q_rows, h * fd : (h + 1) * fd]
                 k = kv_buf[at, :, h * fd : (h + 1) * fd]
                 v = kv_buf[at, :, (fh + h) * fd : (fh + h + 1) * fd]
-                own = jnp.sum(
-                    jnp.where(row_id == col_id, gates_ref[h : h + 1, block_cols(2 * couple + b)], 0.0),
-                    axis=1,
-                    keepdims=True,
-                )
                 logits = lax.dot_general(query, k, NT, preferred_element_type=jnp.float32) * fd ** (-0.5)
-                logits = logits + own - gates_ref[h : h + 1, block_cols(at)]
+                logits = logits + gate_col[b, h] - gates_buf[h : h + 1, block_cols(at)]
                 if first:
                     logits = jnp.where(causal, logits, -jnp.inf)
                 top_new = jnp.max(logits, axis=-1, keepdims=True)
@@ -925,8 +1023,6 @@
             settle(other)
             mix_copy(depth).start()
 
-        outs.relay(2)
-
         def past(i, _):
             q = lax.div(i, 2)
             b = jnp.where(lax.rem(i, 2) == 0, fox_of(q) - 2 * q, 1 - (fox_of(q) - 2 * q))
@@ -950,7 +1046,7 @@
         lax.fori_loop(0, 2 * couple, past, 0)
         settle(mine)
         mix_own(depth)
-        for k in range(3, n):
+        for k in range(2, n):
             outs.relay(k)
         mix_in(0).wait_recv()
         mix_copy(depth).wait_send()
@@ -959,7 +1055,12 @@
 
     @pl.when(is_ret)
     def _():
+        w_relay(ret_arrays, [1] + far)
+        after_tokens()
+        tok_ready(False)
+        normalize(other)
         w_relay(ret_arrays, [n - 1])
+        outs.relay(1)
         w_arrive(ret_arrays)
         proj_buf[:, :ret_wide] = jnp.dot(
             norm_buf[...], w_buf[:, :ret_wide], preferred_element_type=jnp.float32
@@ -997,7 +1098,7 @@
             gap = ((couple - 1 - q) * 2 * rows).astype(jnp.float32)
             return tuple(entering[h] + jnp.exp(lone + gap * decay_ref[h]) * sum_buf[q, h] for h in range(hr))
 
-        entering = tuple(jnp.exp(lone + offset * decay_ref[h]) * state_ref[h] for h in range(hr))
+        entering = tuple(jnp.exp(lone + offset * decay_ref[h]) * state_buf[h] for h in range(hr))
         entering = lax.fori_loop(0, couple, gather, entering)
         second = tuple(jnp.exp(lone + float(rows) * decay_ref[h]) * entering[h] + early[h] for h in range(hr))
 
@@ -1023,7 +1124,7 @@
                 center = raw - jnp.mean(raw, axis=-1, keepdims=True)
                 variance = jnp.mean(center * center, axis=-1, keepdims=True)
                 cols = slice(h * vd, (h + 1) * vd)
-                mix_pair[b, :, cols] = (center * lax.rsqrt(variance + epsilon) * hgain_ref[:, cols]).astype(
+                mix_pair[b, :, cols] = (center * lax.rsqrt(variance + epsilon) * hgain_buf[:, cols]).astype(
                     jnp.bfloat16
                 )
 
@@ -1065,7 +1166,7 @@
         cols = piece_cols(piece)
         at = (d - 1) * pieces + piece
         return rdma(
-            pair_sum.at[slot(to), cols], rs_buf.at[d - 1, :, cols], rs_s.at[at], rs_r.at[at], tp=2 * to + parity
+            pair_sum.at[slot(to), cols], far_ref.at[d - 1, :, cols], rs_s.at[at], rs_r.at[at], tp=2 * to + parity
         )
 
     def project(piece):
@@ -1103,12 +1204,9 @@
     reduce(order(jnp.int32(n - 1)))
 
     own = slot(pair)
-    summed = rs_send[parity, own, :].astype(jnp.float32) + pair_buf[own, :].astype(jnp.float32)
-    for d in range(1, half):
-        for piece in range(pieces):
-            rs_copy(d, piece).wait_recv()
-        summed = summed + rs_buf[d - 1].astype(jnp.float32)
-    out_ref[...] = summed.astype(jnp.bfloat16)
+    near_buf[...] = rs_send[parity, own, :].astype(jnp.float32) + pair_buf[own, :].astype(jnp.float32)
+    near_copy = pltpu.make_async_copy(near_buf, near_ref, near_sem)
+    near_copy.start()
 
     for m in range(chunks):
         tok_z(m).wait_send()
@@ -1117,11 +1215,17 @@
                 tok_x(own_half, m, d).wait_send()
             for d in range(half):
                 tok_c(own_half, m, d).wait_send()
-    send_weights(lambda copy: copy.wait_send())
+
+    def sent(copy):
+        copy.wait_send()
+
+    send_weights(fox_arrays, sent)
+    send_weights(ret_arrays, sent)
 
     def sides(arrays):
         for c in arrays:
             for k in range(1, n):
+                w_pass(c, toward(k), sent)
                 for d in range(1, n_grp):
                     w_side(c, toward(k), d).wait_send()
 
@@ -1138,6 +1242,10 @@
         for d in range(1, half):
             rs_copy(d, piece).wait_send()
     outs.finish()
+    near_copy.wait()
+    for d in range(1, half):
+        for piece in range(pieces):
+            rs_copy(d, piece).wait_recv()
 
 
 def paired(n, n_tp, n_grp, inputs):
@@ -1153,23 +1261,32 @@
     wide = max(3 * fh * fd, 2 * hr * dk + hr * vd)
     half = n_tp // 2
     block = rows // n_tp
-    chunks = 2
+    chunks = 4
     count = 5
     couples = n // 2
     dma = pltpu.SemaphoreType.DMA
     far = max(half - 1, 1)
     side = max(n_grp - 1, 1) * n
-    vmem = pl.BlockSpec(memory_space=pltpu.VMEM)
     smem = pl.BlockSpec(memory_space=pltpu.SMEM)
     hbm = pl.BlockSpec(memory_space=pl.ANY)
     bf16, f32 = jnp.bfloat16, jnp.float32
     size = (n, n_tp, n_grp, hr, dk, vd, fh, fd, chunks)
-    return pl.pallas_call(
+    near, other = pl.pallas_call(
         functools.partial(pair_kernel, size),
-        out_shape=jax.ShapeDtypeStruct((block, columns), bf16),
-        in_specs=[hbm, vmem, vmem, vmem, hbm, hbm, hbm, hbm, smem, vmem, vmem, vmem, hbm, hbm],
-        out_specs=vmem,
+        out_shape=(
+            jax.ShapeDtypeStruct((block, columns), f32),
+            jax.ShapeDtypeStruct((far, block, columns), bf16),
+        ),
+        in_specs=[hbm] * 8 + [smem] + [hbm] * 5,
+        out_specs=(hbm, hbm),
         scratch_shapes=[
+            pltpu.VMEM((1, n_tp * feats), f32),
+            pltpu.VMEM((hr * dk, shard), bf16),
+            pltpu.VMEM((hr * dk, shard), bf16),
+            pltpu.VMEM((hr, dk, vd), f32),
+            pltpu.VMEM((1, hr * vd), f32),
+            pltpu.VMEM((fh, n * rows), f32),
+            pltpu.VMEM((2, fh, rows, 1), f32),
             pltpu.VMEM((2, n_tp, rows, feats), bf16),
             pltpu.VMEM((shard, 2 * hr * dk), bf16),
             pltpu.VMEM((n * shard, wide), bf16),
@@ -1183,10 +1300,14 @@
             pltpu.VMEM((2, rows // 2, columns), bf16),
             pltpu.VMEM((rows // 2, columns), bf16),
             pltpu.VMEM((rows // 2, columns), bf16),
-            pltpu.VMEM((far, block, columns), bf16),
+            pltpu.VMEM((block, columns), f32),
             pltpu.VMEM((2, fh, rows, 1), f32),
             pltpu.VMEM((2, fh, rows, 1), f32),
             pltpu.VMEM((2, fh, rows, fd), f32),
+            dma((6,)),
+            dma,
+            pltpu.SemaphoreType.REGULAR,
+            pltpu.SemaphoreType.REGULAR,
             dma((chunks,)),
             dma((chunks,)),
             dma((2 * chunks * far,)),
@@ -1194,7 +1315,7 @@
             dma((2 * chunks * half,)),
             dma((2 * chunks * half,)),
             dma,
-            dma((n * count,)),
+            dma((2 * n * count,)),
             dma((n * count,)),
             dma((side * count,)),
             dma((side * count,)),
@@ -1236,6 +1357,9 @@
         inputs[12],
         inputs[13],
     )
+    for d in range(half - 1):
+        near = near + other[d].astype(f32)
+    return near.astype(bf16)
 
 
 def pairs_fit(n, n_tp, n_grp, inputs):

time: 57 us -> 54.3 us (0.953)
  the two profiles are of different devices: /device:TPU:0 before, /device:TPU:25 now
where the time goes in v2:
time: 54.3 us; the launch traced here: 54.1 us
  Pallas kernels  52.2 us (96%)
  other arithmetic  1.86 us (3%)
    pallas_call x1, Pallas kernels, paired(): pl.pallas_call(functools.partial(pair_kernel, size), out_shape=(jax.Shape...  52.2 us
    convert_element_type x1, other arithmetic, paired(): return near.astype(bf16)  1.86 us

profile of v2, /device:TPU:25, one launch (start us, length us, event | category | flops | bytes accessed | tf_op | source)
XLA Modules:
  0.0 54.1 jit_solution(10907228796590751875)
XLA Ops:
  0.0 52.2 %layer.1 = (f32[64,2048]{1,0:T(8,128)}, bf16[1,64,2048]{2,1,0:T(8,128)(2,1)}) custom-call(bf16[256,512]{1,0:T(8,128)(2,1)} %tok_ref.1, f32[1,2048]{1,0:T(1,128)} %bitcast.10, bf16[64,512]{1,0:T(8,128)(2,1)} %bitcast.8, bf16[64,512]{1,0:T(8,128)(2,1)} %bitcast.9, bf16[512,128]{1,0:T(8,128)(2,1)} %wrv_ref.1, bf16[512,128]{1,0:T(8,128)(2,1)} %wfq_ref.1, ...), custom_call_target="tpu_custom_call" | custom-call | tf_op jit(solution)/shard_map/layer/pallas_call | solution.py:1274
  52.3 1.9 %fusion = bf16[64,2048]{1,0:T(8,128)(2,1)} fusion(f32[64,2048]{1,0:T(8,128)} %get-tuple-element.7, bf16[1,64,2048]{2,1,0:T(8,128)(2,1)} %get-tuple-element.8), kind=kLoop, calls=%fused_computation.1 | loop fusion | flops 393216 | bytes 1048576 | tf_op jit(solution)/shard_map/convert_element_type | solution.py:1362

commit v3 on v2

--- a/solution.py
+++ b/solution.py
@@ -8,6 +8,7 @@
 from jax.sharding import PartitionSpec as P
 
 epsilon = 1e-06
+lanes = 128
 highest = lax.Precision.HIGHEST
 NT = (((1,), (1,)), ((), ()))
 TN = (((0,), (0,)), ((), ()))
@@ -529,12 +530,11 @@
     near_ref,
     far_ref,
     gain_buf,
-    wq_buf,
-    wk_buf,
+    wqk_buf,
     state_buf,
     hgain_buf,
     gates_buf,
-    gate_col,
+    gate_buf,
     tok_buf,
     qk_own,
     w_buf,
@@ -548,19 +548,15 @@
     rs_send,
     pair_buf,
     pair_sum,
-    near_buf,
     top_buf,
     total_buf,
     weighted_buf,
     in_sem,
-    near_sem,
     above_sem,
     below_sem,
-    tz_s,
+    t_s,
     tz_r,
-    tx_s,
     tx_r,
-    tc_s,
     tc_r,
     t_loc,
     w_s,
@@ -568,6 +564,11 @@
     wy_s,
     wy_r,
     w_loc,
+    o_s,
+    o_r,
+    oy_s,
+    oy_r,
+    o_loc,
     kv_s,
     kv_r,
     sum_s,
@@ -578,7 +579,6 @@
     pair_r,
     rs_s,
     rs_r,
-    *out_sems,
 ):
     n, n_tp, n_grp, hr, dk, vd, fh, fd, chunks = size
     me, t, g = lax.axis_index("sp"), lax.axis_index("tp"), lax.axis_index("grp")
@@ -624,25 +624,20 @@
     def _():
         greet(sp=me - 1)
 
+    def drained(sem, ref):
+        pltpu.make_async_copy(ref, ref, sem).wait()
+
+    width = hr * dk
+    pltpu.make_async_copy(wq_ref, wqk_buf.at[:width], in_sem.at[0]).start()
+    pltpu.make_async_copy(wk_ref, wqk_buf.at[width:], in_sem.at[0]).start()
     brought = [
-        pltpu.make_async_copy(src, dst, in_sem.at[i])
+        pltpu.make_async_copy(src, dst, in_sem.at[i + 1])
         for i, (src, dst) in enumerate(
-            (
-                (wq_ref, wq_buf),
-                (wk_ref, wk_buf),
-                (gain_ref, gain_buf),
-                (state_ref, state_buf),
-                (hgain_ref, hgain_buf),
-                (gates_ref, gates_buf),
-            )
+            ((gain_ref, gain_buf), (state_ref, state_buf), (hgain_ref, hgain_buf), (gates_ref, gates_buf))
         )
     ]
     for copy in brought:
         copy.start()
-    for copy in brought[:2]:
-        copy.wait()
-    turned = jnp.concatenate((wq_buf[...], wk_buf[...]), axis=0).astype(jnp.float32)
-    qk_own[...] = turned.T.astype(jnp.bfloat16)
 
     pl.semaphore_wait(barrier, half + n_grp - 1 + has_up.astype(jnp.int32) + has_down.astype(jnp.int32))
 
@@ -685,48 +680,36 @@
         return tok_buf.at[h, src, pl.ds(m * slab, slab)]
 
     def tok_z(m):
-        return rdma(own_tok(m), tok_at(mine, m, t), tz_s.at[m], tz_r.at[m], sp=partner)
+        return rdma(own_tok(m), tok_at(mine, m, t), t_s, tz_r.at[m], sp=partner)
 
     def tok_z_in(m):
         here = tok_at(other, m, t)
-        return rdma(here, here, tz_s.at[m], tz_r.at[m], sp=partner)
+        return rdma(here, here, t_s, tz_r.at[m], sp=partner)
 
     def x_sem(own, m, d):
-        return ((0 if own else 1) * chunks + m) * max(half - 1, 1) + d - 1
+        return (0 if own else 1 + m) * max(half - 1, 1) + d - 1
 
     def tok_x(own, m, d):
-        at = x_sem(own, m, d)
         h = mine if own else other
         src = own_tok(m) if own else tok_at(h, m, t)
-        return rdma(src, tok_at(h, m, t), tx_s.at[at], tx_r.at[at], tp=2 * lax.rem(pair + d, half) + parity)
+        return rdma(src, tok_at(h, m, t), t_s, tx_r.at[x_sem(own, m, d)], tp=2 * lax.rem(pair + d, half) + parity)
 
     def tok_x_in(own, m, d):
-        at = x_sem(own, m, d)
         src = 2 * lax.rem(pair + half - d, half) + parity
-        here = tok_at(mine if own else other, m, src)
-        return rdma(here, here, tx_s.at[at], tx_r.at[at], tp=src)
-
-    def c_sem(own, m, d):
-        return ((0 if own else 1) * chunks + m) * half + d
+        here = tok_buf.at[mine, src] if own else tok_at(other, m, src)
+        return rdma(here, here, t_s, tx_r.at[x_sem(own, m, d)], tp=src)
 
     def tok_c(own, m, d):
-        at = c_sem(own, m, d)
         h = mine if own else other
         src = 2 * lax.rem(pair + half - d, half) + parity
         there = tok_at(h, m, src)
         here = own_tok(m) if own and d == 0 else there
-        return rdma(here, there, tc_s.at[at], tc_r.at[at], tp=2 * pair + 1 - parity)
-
-    def tok_c_in(own, m, d):
-        at = c_sem(own, m, d)
-        src = 2 * lax.rem(pair + half - d, half) + 1 - parity
-        here = tok_at(mine if own else other, m, src)
-        return rdma(here, here, tc_s.at[at], tc_r.at[at], tp=2 * pair + 1 - parity)
+        return rdma(here, there, t_s, tc_r.at[0 if own else 1], tp=2 * pair + 1 - parity)
 
     tok_local = pltpu.make_async_copy(tok_ref, tok_buf.at[mine, t], t_loc)
 
-    for m in range(chunks):
-        for d in range(1, half):
+    for d in range(1, half):
+        for m in range(chunks):
             tok_x(True, m, d).start()
 
     owns = [wfk_ref, wfv_ref, wfq_ref, wrv_ref, qk_own]
@@ -746,36 +729,34 @@
         start = pl.multiple_of(src * shard + part * step, step)
         return w_buf.at[pl.ds(start, step), starts[c][0] : starts[c][1]]
 
-    def w_sem(c, src, up):
-        return ((0 if up else n) + src) * count + c
-
-    def w_send(c, to, up):
+    local_at = {c: c - group[0] for group in (fox_arrays, ret_arrays) for c in group}
+
+    def w_recv(c, src):
+        return w_r.at[src * len(fox_arrays) + local_at[c]]
+
+    def w_send(c, to):
         here = owns[c].at[pl.ds(pl.multiple_of(g * step, step), step)]
-        return rdma(here, w_at(c, me, g), w_s.at[w_sem(c, me, up)], w_r.at[me * count + c], sp=to)
-
-    def w_on(c, src, to, up):
+        return rdma(here, w_at(c, me, g), w_s.at[c], w_recv(c, me), sp=to)
+
+    def w_on(c, src, to):
         here = w_at(c, src, g)
-        return rdma(here, here, w_s.at[w_sem(c, src, up)], w_r.at[src * count + c], sp=to)
+        return rdma(here, here, w_s.at[c], w_recv(c, src), sp=to)
 
     def w_in(c, src):
         here = w_at(c, src, g)
-        return rdma(here, here, w_s.at[src * count + c], w_r.at[src * count + c], sp=src)
+        return rdma(here, here, w_s.at[c], w_recv(c, src), sp=src)
 
     def w_side(c, src, d):
-        at = ((d - 1) * n + src) * count + c
         here = w_at(c, src, g)
-        return rdma(here, here, wy_s.at[at], wy_r.at[at], grp=lax.rem(g + d, n_grp))
-
-    def w_side_in(c, src, d):
-        at = ((d - 1) * n + src) * count + c
-        part = lax.rem(g + n_grp - d, n_grp)
-        here = w_at(c, src, part)
-        return rdma(here, here, wy_s.at[at], wy_r.at[at], grp=part)
+        return rdma(here, here, wy_s.at[local_at[c]], wy_r.at[local_at[c]], grp=lax.rem(g + d, n_grp))
+
+    def w_several(c, pieces):
+        return w_buf.at[: pieces * step, starts[c][0] : starts[c][1]]
 
     def w_local(c):
         start = pl.multiple_of(me * shard, shard)
         return pltpu.make_async_copy(
-            owns[c], w_buf.at[pl.ds(start, shard), starts[c][0] : starts[c][1]], w_loc.at[c]
+            owns[c], w_buf.at[pl.ds(start, shard), starts[c][0] : starts[c][1]], w_loc.at[local_at[c]]
         )
 
     fox_up = jnp.where(is_ret & (mine == 0), partner, fox_of(couple + 1))
@@ -783,26 +764,36 @@
     ret_up = jnp.where(is_fox & (mine == 0), partner, ret_of(couple + 1))
     ret_down = jnp.where(is_fox & (mine == 1), partner, jnp.where(couple >= 1, ret_of(jnp.maximum(couple - 1, 0)), -1))
 
-    def send_weights(arrays, act):
+    def send_weights(arrays):
         up, down = (fox_up, fox_down) if arrays[0] in fox_arrays else (ret_up, ret_down)
         for c in arrays:
 
             @pl.when(up < n)
             def _(c=c):
-                act(w_send(c, up, True))
+                w_send(c, up).start()
 
             @pl.when(down >= 0)
             def _(c=c):
-                act(w_send(c, down, False))
-
-    def start(copy):
-        copy.start()
-
-    send_weights((0, 1), start)
+                w_send(c, down).start()
+
+    def sends_from(p, arrays):
+        q, b = p // 2, p % 2
+        plane = (lambda i: 2 * i + 1 - i % 2) if arrays[0] in fox_arrays else (lambda i: 2 * i + i % 2)
+        uses = plane(q) == p
+        up = p + 1 if not uses and b == 0 else plane(q + 1)
+        down = p - 1 if not uses and b == 1 else (plane(q - 1) if q else -1)
+        passes = ((p if up < n else 0) + (n - 1 - p if down >= 0 else 0)) if uses else 0
+        return (up < n) + (down >= 0) + passes
+
+    send_weights((0, 1))
     for m in range(chunks):
         tok_z(m).start()
         tok_c(True, m, 0).start()
-    send_weights((2,), start)
+    send_weights((2,))
+    meet_far()
+    send_weights((3,))
+    drained(in_sem.at[0], wqk_buf)
+    qk_own[...] = wqk_buf[...].astype(jnp.float32).T.astype(jnp.bfloat16)
     tok_local.start()
 
     @pl.when(is_fox)
@@ -812,43 +803,88 @@
 
     @pl.when(is_ret)
     def _():
-        for c in ret_arrays:
-            w_local(c).start()
+        w_local(3).start()
 
     depth = mix_buf.shape[1] // 2
     out_cols = ret_out_ref.shape[1]
 
-    def out_place(src, c, first, rows_):
-        start = pl.multiple_of(c * depth + first, rows_)
-        return wout_buf.at[pl.ds(start, rows_), pl.ds(pl.multiple_of(src * out_cols, out_cols), out_cols)]
-
-    outs = LineGather([ret_out_ref, fox_out_ref], out_place, out_sems, n, n_grp, me, g)
-
-    def w_pass(c, src, act):
+    out_step = depth // n_grp
+    out_refs = [ret_out_ref, fox_out_ref]
+
+    def out_cols_of(src):
+        return pl.ds(pl.multiple_of(src * out_cols, out_cols), out_cols)
+
+    def out_at(c, src):
+        return wout_buf.at[pl.ds(pl.multiple_of(c * depth + g * out_step, out_step), out_step), out_cols_of(src)]
+
+    def out_both(src):
+        return wout_buf.at[: 2 * out_step, out_cols_of(src)]
+
+    def out_hop(c, src, to, first):
+        here = out_refs[c].at[pl.ds(pl.multiple_of(g * out_step, out_step), out_step)] if first else out_at(c, src)
+        return rdma(here, out_at(c, src), o_s, o_r.at[src], sp=to)
+
+    def out_local(c):
+        return pltpu.make_async_copy(out_refs[c], wout_buf.at[c * depth : (c + 1) * depth, out_cols_of(me)], o_loc)
+
+    def out_begin():
+        for c in range(2):
+
+            @pl.when(has_up)
+            def _(c=c):
+                out_hop(c, me, me + 1, True).start()
+
+            @pl.when(has_down)
+            def _(c=c):
+                out_hop(c, me, me - 1, True).start()
+
+            out_local(c).start()
+
+    def out_relay(i):
+        for src, to in ((me - i, me + 1), (me + i, me - 1)):
+
+            @pl.when((src >= 0) & (src < n))
+            def _(src=src, to=to):
+                both = out_both(src)
+                rdma(both, both, o_s, o_r.at[src], sp=src).wait_recv()
+                for c in range(2):
+
+                    @pl.when((to >= 0) & (to < n))
+                    def _(c=c):
+                        out_hop(c, src, to, False).start()
+
+                    for d in range(1, n_grp):
+                        here = out_at(c, src)
+                        at = (d - 1) * n + src
+                        rdma(here, here, oy_s, oy_r.at[at], grp=lax.rem(g + d, n_grp)).start()
+
+    def out_arrive(src):
+        for d in range(1, n_grp):
+            drained(oy_r.at[(d - 1) * n + src], out_both(src))
+
+    def w_pass(c, src):
         up, down = (fox_up, fox_down) if c in fox_arrays else (ret_up, ret_down)
 
         @pl.when((src < me) & (up < n))
         def _():
-            act(w_on(c, src, up, True))
+            w_on(c, src, up).start()
 
         @pl.when((src > me) & (down >= 0))
         def _():
-            act(w_on(c, src, down, False))
+            w_on(c, src, down).start()
 
     def w_relay(arrays, ks):
-        for k in ks:
+        for i in ks:
             for c in arrays:
-                w_in(c, toward(k)).wait_recv()
-                w_pass(c, toward(k), start)
+                w_in(c, toward(i)).wait_recv()
+                w_pass(c, toward(i))
                 for d in range(1, n_grp):
-                    w_side(c, toward(k), d).start()
+                    w_side(c, toward(i), d).start()
 
     def w_arrive(arrays):
         for c in arrays:
             w_local(c).wait()
-            for k in range(1, n):
-                for d in range(1, n_grp):
-                    w_side_in(c, toward(k), d).wait_recv()
+            drained(wy_r.at[local_at[c]], w_several(c, (n - 1) * (n_grp - 1)))
 
     def normalize(h):
         squares = jnp.zeros((rows, 1), jnp.float32)
@@ -864,10 +900,11 @@
 
     far = list(range(2, n - 1))
 
-    def tok_own(m):
+    def tok_own():
         for d in range(1, half):
-            tok_x_in(True, m, d).wait_recv()
-            tok_c(True, m, d).start()
+            tok_x_in(True, 0, d).wait_recv()
+            for m in range(chunks):
+                tok_c(True, m, d).start()
 
     def tok_swap(m):
         tok_z_in(m).wait_recv()
@@ -883,29 +920,31 @@
     def tok_ready(own):
         if own:
             tok_local.wait()
-        for m in range(chunks):
-            for d in range(half):
-                tok_c_in(own, m, d).wait_recv()
-
-    for copy in brought[2:]:
+        drained(tc_r.at[0 if own else 1], tok_buf.at[mine if own else other, :half])
+
+    for copy in brought:
         copy.wait()
 
     @pl.when(is_fox)
     def _():
         w_relay((0, 1), [1, n - 1])
 
-    meet_far()
-    send_weights(ret_arrays, start)
-    outs.start()
-
-    for m in range(chunks):
-        tok_own(m)
+    send_weights((4,))
+    out_begin()
+
+    @pl.when(is_ret)
+    def _():
+        w_local(4).start()
+
+    tok_swap(0)
+    tok_own()
+    for m in range(1, chunks):
         tok_swap(m)
 
     @pl.when(is_fox)
     def _():
         w_relay((0, 1), far)
-        w_relay((2,), [1])
+        w_relay((2,), [1, n - 1])
 
     tok_ready(True)
     normalize(mine)
@@ -919,7 +958,7 @@
 
     def mix_copy(first):
         return rdma(
-            mix_pair.at[other], mix_buf.at[:, first : first + depth], mix_s.at[0], mix_r.at[0], sp=partner
+            mix_pair.at[other], mix_buf.at[:, first : first + depth], mix_s, mix_r, sp=partner
         )
 
     def mix_own(first):
@@ -927,7 +966,7 @@
 
     def mix_in(first):
         here = mix_buf.at[:, first : first + depth]
-        return rdma(here, here, mix_s.at[0], mix_r.at[0], sp=partner)
+        return rdma(here, here, mix_s, mix_r, sp=partner)
 
     def kv_copy(b, q):
         at = 2 * couple + b
@@ -962,92 +1001,81 @@
             later(lambda q: kv_copy(b, q).start())
 
         after_tokens()
+        w_relay((2,), far)
         w_arrive((0, 1))
         project_kv(mine)
-        w_relay((2,), [n - 1] + far)
         tok_ready(False)
         normalize(other)
         project_kv(other)
-        outs.relay(1)
         w_arrive((2,))
         proj_buf[:, : fh * fd] = jnp.dot(
             norm_buf[...], w_buf[:, q_at:fox_wide], preferred_element_type=jnp.float32
         ).astype(jnp.bfloat16)
+        out_relay(1)
 
         def block_cols(at):
             return pl.ds(pl.multiple_of(at * rows, rows), rows)
+
+        def rep_cols(x, wide):
+            return jnp.concatenate([x] * (wide // lanes), axis=1)
 
         for b in range(2):
             for h in range(fh):
                 own = jnp.where(row_id == col_id, gates_buf[h : h + 1, block_cols(2 * couple + b)], 0.0)
-                gate_col[b, h] = jnp.sum(own, axis=1, keepdims=True)
-
-        def attend(b, at, first):
-            q_rows = pl.ds(pl.multiple_of(b * rows, rows), rows)
+                gate_buf[h, b * rows : (b + 1) * rows] = jnp.broadcast_to(
+                    jnp.sum(own, axis=1, keepdims=True), (rows, lanes)
+                )
+
+        def attend(at, top_row, first, offset):
+            size_ = 2 * rows - top_row
+            here = slice(top_row, 2 * rows)
             for h in range(fh):
-                query = proj_buf[q_rows, h * fd : (h + 1) * fd]
+                query = proj_buf[here, h * fd : (h + 1) * fd]
                 k = kv_buf[at, :, h * fd : (h + 1) * fd]
                 v = kv_buf[at, :, (fh + h) * fd : (fh + h + 1) * fd]
                 logits = lax.dot_general(query, k, NT, preferred_element_type=jnp.float32) * fd ** (-0.5)
-                logits = logits + gate_col[b, h] - gates_buf[h : h + 1, block_cols(at)]
-                if first:
-                    logits = jnp.where(causal, logits, -jnp.inf)
-                top_new = jnp.max(logits, axis=-1, keepdims=True)
+                logits = logits + rep_cols(gate_buf[h, here], rows) - gates_buf[h : h + 1, block_cols(at)]
+                if offset is not None:
+                    row = lax.broadcasted_iota(jnp.int32, (size_, rows), 0)
+                    col = lax.broadcasted_iota(jnp.int32, (size_, rows), 1)
+                    logits = jnp.where(col <= row, logits, -jnp.inf)
+                top_new = jnp.broadcast_to(jnp.max(logits, axis=-1, keepdims=True), (size_, lanes))
                 if not first:
-                    top = top_buf[b, h]
+                    top = top_buf[h, here]
                     top_new = jnp.maximum(top, top_new)
-                p = jnp.exp(logits - top_new)
-                total = jnp.sum(p, axis=-1, keepdims=True)
+                p = jnp.exp(logits - rep_cols(top_new, rows))
+                total = jnp.broadcast_to(jnp.sum(p, axis=-1, keepdims=True), (size_, lanes))
                 weighted = jnp.dot(p.astype(jnp.bfloat16), v, preferred_element_type=jnp.float32)
                 if not first:
                     rescale = jnp.exp(top - top_new)
-                    total = total_buf[b, h] * rescale + total
-                    weighted = weighted_buf[b, h] * rescale + weighted
-                top_buf[b, h] = top_new
-                total_buf[b, h] = total
-                weighted_buf[b, h] = weighted
-
-        def settle(b):
-            for h in range(fh):
-                mix_pair[b, :, h * fd : (h + 1) * fd] = (weighted_buf[b, h] / total_buf[b, h]).astype(jnp.bfloat16)
-
-        def diagonal(b, _):
-            attend(b, 2 * couple + b, True)
-            return 0
-
-        lax.fori_loop(0, 2, diagonal, 0)
-        attend(1, 2 * couple, False)
-
-        @pl.when(couple == 0)
-        def _():
-            settle(other)
-            mix_copy(depth).start()
+                    total = total_buf[h, here] * rescale + total
+                    weighted = weighted_buf[h, here] * rescale[:, :fd] + weighted
+                top_buf[h, here] = top_new
+                total_buf[h, here] = total
+                weighted_buf[h, here] = weighted
+
+        attend(2 * couple, 0, True, 0)
+        attend(2 * couple + 1, rows, False, 0)
 
         def past(i, _):
             q = lax.div(i, 2)
             b = jnp.where(lax.rem(i, 2) == 0, fox_of(q) - 2 * q, 1 - (fox_of(q) - 2 * q))
             at = 2 * q + b
             kv_in(at).wait_recv()
-
-            def both(j, _):
-                row_half = jnp.where(j == 0, other, mine)
-                attend(row_half, at, False)
-
-                @pl.when((j == 0) & (i == 2 * couple - 1))
-                def _():
-                    settle(other)
-                    mix_copy(depth).start()
-
-                return 0
-
-            lax.fori_loop(0, 2, both, 0)
+            attend(at, 0, False, None)
             return 0
 
         lax.fori_loop(0, 2 * couple, past, 0)
-        settle(mine)
+        for b in range(2):
+            at = slice(b * rows, (b + 1) * rows)
+            for h in range(fh):
+                mix_pair[b, :, h * fd : (h + 1) * fd] = (
+                    weighted_buf[h, at] / total_buf[h, at, :fd]
+                ).astype(jnp.bfloat16)
+        mix_copy(depth).start()
         mix_own(depth)
         for k in range(2, n):
-            outs.relay(k)
+            out_relay(k)
         mix_in(0).wait_recv()
         mix_copy(depth).wait_send()
         later(lambda q: kv_copy(0, q).wait_send())
@@ -1060,7 +1088,7 @@
         tok_ready(False)
         normalize(other)
         w_relay(ret_arrays, [n - 1])
-        outs.relay(1)
+        out_relay(1)
         w_arrive(ret_arrays)
         proj_buf[:, :ret_wide] = jnp.dot(
             norm_buf[...], w_buf[:, :ret_wide], preferred_element_type=jnp.float32
@@ -1089,7 +1117,7 @@
         for h in range(hr):
             sum_buf[couple, h] = jnp.exp(lone + float(rows) * decay_ref[h]) * early[h] + summary(1, h)
         later(lambda q: sum_copy(q).start())
-        outs.relay(2)
+        out_relay(2)
 
         offset = (couple * 2 * rows).astype(jnp.float32)
 
@@ -1137,7 +1165,7 @@
         lax.fori_loop(0, 2, block, 0)
         mix_own(0)
         for k in range(3, n):
-            outs.relay(k)
+            out_relay(k)
         mix_in(depth).wait_recv()
         mix_copy(0).wait_send()
         later(lambda q: sum_copy(q).wait_send())
@@ -1156,7 +1184,7 @@
         return rdma(
             rs_send.at[1 - parity, :, cols],
             pair_buf.at[:, cols],
-            pair_s.at[piece],
+            pair_s,
             pair_r.at[piece],
             tp=t + 1 - 2 * parity,
         )
@@ -1164,9 +1192,12 @@
     def rs_copy(d, piece):
         to = lax.rem(pair + d, half)
         cols = piece_cols(piece)
-        at = (d - 1) * pieces + piece
         return rdma(
-            pair_sum.at[slot(to), cols], far_ref.at[d - 1, :, cols], rs_s.at[at], rs_r.at[at], tp=2 * to + parity
+            pair_sum.at[slot(to), cols],
+            far_ref.at[d - 1, :, cols],
+            rs_s.at[d - 1],
+            rs_r.at[d - 1],
+            tp=2 * to + parity,
         )
 
     def project(piece):
@@ -1190,44 +1221,39 @@
         rising = jnp.where(i <= n - 1 - me, me + i, n - 1 - i)
         return jnp.where(lower, rising, falling)
 
-    for c in range(2):
-        outs.local(c).wait()
+    drained(o_loc, wout_buf.at[:, out_cols_of(me)])
     project(me)
 
-    def out_step(i, _):
-        outs.arrive_shard(order(i), (0, 1))
+    def turn(i, _):
+        out_arrive(order(i))
         project(order(i))
         reduce(order(i - 1))
         return 0
 
-    lax.fori_loop(1, n, out_step, 0)
+    lax.fori_loop(1, n, turn, 0)
     reduce(order(jnp.int32(n - 1)))
 
     own = slot(pair)
-    near_buf[...] = rs_send[parity, own, :].astype(jnp.float32) + pair_buf[own, :].astype(jnp.float32)
-    near_copy = pltpu.make_async_copy(near_buf, near_ref, near_sem)
-    near_copy.start()
-
-    for m in range(chunks):
-        tok_z(m).wait_send()
-        for own_half in (True, False):
-            for d in range(1, half):
-                tok_x(own_half, m, d).wait_send()
-            for d in range(half):
-                tok_c(own_half, m, d).wait_send()
-
-    def sent(copy):
-        copy.wait_send()
-
-    send_weights(fox_arrays, sent)
-    send_weights(ret_arrays, sent)
+    near_ref[...] = rs_send[parity, own, :].astype(jnp.float32) + pair_buf[own, :].astype(jnp.float32)
+
+    slabs = rows * (2 * n_tp - 1) // (2 * n_tp)
+    drained(t_s, tok_buf.at[:, :, :slabs])
+    for p in range(n):
+
+        @pl.when(me == p)
+        def _(p=p):
+            for arrays in (fox_arrays, ret_arrays):
+                for c in arrays:
+                    if sends_from(p, arrays):
+                        drained(w_s.at[c], w_several(c, sends_from(p, arrays)))
+            hops = 2 * ((p + 1 if p + 1 < n else 0) + (n - p if p else 0))
+            drained(o_s, wout_buf.at[: hops * out_step // n])
+
+    drained(oy_s, wout_buf.at[: 2 * (n - 1) * (n_grp - 1) * out_step // n])
 
     def sides(arrays):
         for c in arrays:
-            for k in range(1, n):
-                w_pass(c, toward(k), sent)
-                for d in range(1, n_grp):
-                    w_side(c, toward(k), d).wait_send()
+            drained(wy_s.at[local_at[c]], w_several(c, (n - 1) * (n_grp - 1)))
 
     @pl.when(is_fox)
     def _():
@@ -1237,15 +1263,11 @@
     def _():
         sides(ret_arrays)
 
-    for piece in range(pieces):
-        pair_copy(piece).wait_send()
-        for d in range(1, half):
-            rs_copy(d, piece).wait_send()
-    outs.finish()
-    near_copy.wait()
+    drained(pair_s, pair_buf)
     for d in range(1, half):
-        for piece in range(pieces):
-            rs_copy(d, piece).wait_recv()
+        drained(rs_s.at[d - 1], pair_sum.at[:block])
+    for d in range(1, half):
+        drained(rs_r.at[d - 1], far_ref.at[d - 1])
 
 
 def paired(n, n_tp, n_grp, inputs):
@@ -1262,31 +1284,27 @@
     half = n_tp // 2
     block = rows // n_tp
     chunks = 4
-    count = 5
     couples = n // 2
     dma = pltpu.SemaphoreType.DMA
     far = max(half - 1, 1)
     side = max(n_grp - 1, 1) * n
+    vmem = pl.BlockSpec(memory_space=pltpu.VMEM)
     smem = pl.BlockSpec(memory_space=pltpu.SMEM)
     hbm = pl.BlockSpec(memory_space=pl.ANY)
     bf16, f32 = jnp.bfloat16, jnp.float32
     size = (n, n_tp, n_grp, hr, dk, vd, fh, fd, chunks)
     near, other = pl.pallas_call(
         functools.partial(pair_kernel, size),
-        out_shape=(
-            jax.ShapeDtypeStruct((block, columns), f32),
-            jax.ShapeDtypeStruct((far, block, columns), bf16),
-        ),
+        out_shape=(pltpu.VMEM((block, columns), f32), pltpu.VMEM((far, block, columns), bf16)),
         in_specs=[hbm] * 8 + [smem] + [hbm] * 5,
-        out_specs=(hbm, hbm),
+        out_specs=(vmem, vmem),
         scratch_shapes=[
             pltpu.VMEM((1, n_tp * feats), f32),
-            pltpu.VMEM((hr * dk, shard), bf16),
-            pltpu.VMEM((hr * dk, shard), bf16),
+            pltpu.VMEM((2 * hr * dk, shard), bf16),
             pltpu.VMEM((hr, dk, vd), f32),
             pltpu.VMEM((1, hr * vd), f32),
             pltpu.VMEM((fh, n * rows), f32),
-            pltpu.VMEM((2, fh, rows, 1), f32),
+            pltpu.VMEM((fh, 2 * rows, lanes), f32),
             pltpu.VMEM((2, n_tp, rows, feats), bf16),
             pltpu.VMEM((shard, 2 * hr * dk), bf16),
             pltpu.VMEM((n * shard, wide), bf16),
@@ -1300,42 +1318,37 @@
             pltpu.VMEM((2, rows // 2, columns), bf16),
             pltpu.VMEM((rows // 2, columns), bf16),
             pltpu.VMEM((rows // 2, columns), bf16),
-            pltpu.VMEM((block, columns), f32),
-            pltpu.VMEM((2, fh, rows, 1), f32),
-            pltpu.VMEM((2, fh, rows, 1), f32),
-            pltpu.VMEM((2, fh, rows, fd), f32),
-            dma((6,)),
-            dma,
+            pltpu.VMEM((fh, 2 * rows, lanes), f32),
+            pltpu.VMEM((fh, 2 * rows, lanes), f32),
+            pltpu.VMEM((fh, 2 * rows, fd), f32),
+            dma((5,)),
             pltpu.SemaphoreType.REGULAR,
             pltpu.SemaphoreType.REGULAR,
+            dma,
             dma((chunks,)),
-            dma((chunks,)),
-            dma((2 * chunks * far,)),
-            dma((2 * chunks * far,)),
-            dma((2 * chunks * half,)),
-            dma((2 * chunks * half,)),
+            dma(((chunks + 1) * far,)),
+            dma((2,)),
             dma,
-            dma((2 * n * count,)),
-            dma((n * count,)),
-            dma((side * count,)),
-            dma((side * count,)),
-            dma((count,)),
+            dma((5,)),
+            dma((3 * n,)),
+            dma((3,)),
+            dma((3,)),
+            dma((3,)),
+            dma,
+            dma((n,)),
+            dma,
+            dma((side,)),
+            dma,
             dma((2 * couples,)),
             dma((n,)),
             dma((couples,)),
             dma((couples,)),
-            dma((1,)),
-            dma((1,)),
+            dma,
+            dma,
+            dma,
             dma((n,)),
-            dma((n,)),
-            dma((far * n,)),
-            dma((far * n,)),
-            dma((n * 2,)),
-            dma((n * 2,)),
-            dma((n * 2,)),
-            dma((side * 2,)),
-            dma((side * 2,)),
-            dma((2,)),
+            dma((far,)),
+            dma((far,)),
         ],
         compiler_params=pltpu.CompilerParams(
             collective_id=0, has_side_effects=True, vmem_limit_bytes=56 * 1024 * 1024
@@ -1368,12 +1381,12 @@
     shard = inputs[2].shape[0]
     depth, out_cols = inputs[12].shape
     wide = inputs[5].shape[1]
-    lanes = all(w % 128 == 0 for w in (out_cols, wide, 2 * hr * dk, hr * vd, feats, depth))
-    even = n % 2 == 0 and n > 2 and n_tp % 2 == 0
-    tiles = rows % (16 * n_tp) == 0 and rows % 32 == 0 and shard % (16 * n_grp) == 0 and depth % (16 * n_grp) == 0
+    full = all(w % lanes == 0 for w in (out_cols, wide, 2 * hr * dk, hr * vd, feats, depth, rows))
+    even = n % 2 == 0 and n > 2 and n_tp % 2 == 0 and n_grp > 1
+    tiles = rows % (32 * n_tp) == 0 and rows % 32 == 0 and shard % (16 * n_grp) == 0 and depth % (16 * n_grp * n) == 0 and vd <= lanes
     columns = n * out_cols
     held = 8 * rows * n_tp * feats + 2 * n * shard * 3 * wide + 4 * depth * columns + 4 * n * rows * wide + 6 * rows * columns
-    return lanes and even and tiles and depth == wide == hr * vd and held < 40 * 1024 * 1024
+    return full and even and tiles and depth == wide == hr * vd and held < 40 * 1024 * 1024
 
 
 def local(

time: 54.3 us -> 48.3 us (0.89)
  the two profiles are of different devices: /device:TPU:25 before, /device:TPU:17 now
where the time goes in v3:
time: 48.3 us; the launch traced here: 48.1 us
  Pallas kernels  47.3 us (98%)
  other arithmetic  0.75 us (2%)
    pallas_call x1, Pallas kernels, paired(): pl.pallas_call(functools.partial(pair_kernel, size), out_shape=(pltpu.VME...  47.3 us

profile of v3, /device:TPU:17, one launch (start us, length us, event | category | flops | bytes accessed | tf_op | source)
XLA Modules:
  0.0 48.1 jit_solution(1788474000771343395)
XLA Ops:
  0.0 47.3 %layer.1 = (f32[64,2048]{1,0:T(8,128)S(1)}, bf16[1,64,2048]{2,1,0:T(8,128)(2,1)S(1)}) custom-call(bf16[256,512]{1,0:T(8,128)(2,1)} %tok_ref.1, f32[1,2048]{1,0:T(1,128)} %bitcast.10, bf16[64,512]{1,0:T(8,128)(2,1)} %bitcast.8, bf16[64,512]{1,0:T(8,128)(2,1)} %bitcast.9, bf16[512,128]{1,0:T(8,128)(2,1)} %wrv_ref.1, bf16[512,128]{1,0:T(8,128)(2,1)} %wfq_ref.1, ...), custom_call_target="tpu_custom_call" | custom-call | tf_op jit(solution)/shard_map/layer/pallas_call | solution.py:1296
  47.4 0.8 %fusion = bf16[64,2048]{1,0:T(8,128)(2,1)} fusion(f32[64,2048]{1,0:T(8,128)S(1)} %get-tuple-element.7, bf16[1,64,2048]{2,1,0:T(8,128)(2,1)S(1)} %get-tuple-element.8), kind=kLoop, calls=%fused_computation.1 | loop fusion | flops 393216 | bytes 1048576 | tf_op jit(solution)/shard_map/convert_element_type | solution.py:1375

commit v4 on v3

--- a/solution.py
+++ b/solution.py
@@ -535,6 +535,8 @@
     hgain_buf,
     gates_buf,
     gate_buf,
+    within_buf,
+    raw_buf,
     tok_buf,
     qk_own,
     w_buf,
@@ -794,6 +796,7 @@
     send_weights((3,))
     drained(in_sem.at[0], wqk_buf)
     qk_own[...] = wqk_buf[...].astype(jnp.float32).T.astype(jnp.bfloat16)
+    send_weights((4,))
     tok_local.start()
 
     @pl.when(is_fox)
@@ -929,9 +932,6 @@
     def _():
         w_relay((0, 1), [1, n - 1])
 
-    send_weights((4,))
-    out_begin()
-
     @pl.when(is_ret)
     def _():
         w_local(4).start()
@@ -946,6 +946,11 @@
         w_relay((0, 1), far)
         w_relay((2,), [1, n - 1])
 
+    @pl.when(is_ret)
+    def _():
+        w_relay(ret_arrays, [1])
+
+    out_begin()
     tok_ready(True)
     normalize(mine)
 
@@ -1001,17 +1006,17 @@
             later(lambda q: kv_copy(b, q).start())
 
         after_tokens()
-        w_relay((2,), far)
         w_arrive((0, 1))
         project_kv(mine)
         tok_ready(False)
         normalize(other)
         project_kv(other)
+        w_relay((2,), far)
+        out_relay(1)
         w_arrive((2,))
         proj_buf[:, : fh * fd] = jnp.dot(
             norm_buf[...], w_buf[:, q_at:fox_wide], preferred_element_type=jnp.float32
         ).astype(jnp.bfloat16)
-        out_relay(1)
 
         def block_cols(at):
             return pl.ds(pl.multiple_of(at * rows, rows), rows)
@@ -1083,8 +1088,12 @@
 
     @pl.when(is_ret)
     def _():
-        w_relay(ret_arrays, [1] + far)
+        distance = jnp.maximum(row_id - col_id, 0).astype(jnp.float32)
+        key_scale = dk ** (-0.5)
+        for h in range(hr):
+            within_buf[h] = jnp.where(causal, jnp.exp(distance * decay_ref[h]) * key_scale, 0.0)
         after_tokens()
+        w_relay(ret_arrays, far)
         tok_ready(False)
         normalize(other)
         w_relay(ret_arrays, [n - 1])
@@ -1094,29 +1103,46 @@
             norm_buf[...], w_buf[:, :ret_wide], preferred_element_type=jnp.float32
         ).astype(jnp.bfloat16)
         rv_at, rq_at = starts[3][0], starts[4][0]
-        key_scale = dk ** (-0.5)
-        position = lax.broadcasted_iota(jnp.int32, (rows, 1), 0).astype(jnp.float32)
-        distance = jnp.maximum(row_id - col_id, 0).astype(jnp.float32)
         lone = jnp.zeros((dk, vd), jnp.float32)
 
         def part(b, first, wide):
-            return proj_buf[pl.ds(pl.multiple_of(b * rows, rows), rows), first : first + wide]
+            return proj_buf[b * rows : (b + 1) * rows, first : first + wide]
+
+        def split(x, axis):
+            top = x.astype(jnp.bfloat16)
+            rest = x - top.astype(jnp.float32)
+            middle = rest.astype(jnp.bfloat16)
+            low = (rest - middle.astype(jnp.float32)).astype(jnp.bfloat16)
+            return jnp.concatenate((top, middle, low), axis=axis)
 
         def summary(b, h):
+            past_end = rows - 1.0 - lax.broadcasted_iota(jnp.int32, (rows, dk), 0).astype(jnp.float32)
             keys = part(b, rq_at + (hr + h) * dk, dk).astype(jnp.float32) * key_scale
-            trailing = jnp.exp((rows - 1.0 - position) * decay_ref[h])
-            return lax.dot_general(
-                keys * trailing,
-                part(b, rv_at + h * vd, vd).astype(jnp.float32),
+            parts = lax.dot_general(
+                split(keys * jnp.exp(past_end * decay_ref[h]), 1),
+                part(b, rv_at + h * vd, vd),
                 TN,
-                precision=highest,
                 preferred_element_type=jnp.float32,
             )
+            return parts[:dk] + parts[dk : 2 * dk] + parts[2 * dk :]
 
         early = [summary(0, h) for h in range(hr)]
         for h in range(hr):
             sum_buf[couple, h] = jnp.exp(lone + float(rows) * decay_ref[h]) * early[h] + summary(1, h)
         later(lambda q: sum_copy(q).start())
+
+        for b in range(2):
+            for h in range(hr):
+                rk = part(b, rq_at + (hr + h) * dk, dk)
+                rv = part(b, rv_at + h * vd, vd)
+                scores = lax.dot_general(
+                    part(b, rq_at + h * dk, dk), rk, NT, preferred_element_type=jnp.float32
+                )
+                raw_buf[b, h] = jnp.dot(
+                    split(scores * within_buf[h], 1),
+                    jnp.concatenate((rv, rv, rv), axis=0),
+                    preferred_element_type=jnp.float32,
+                )
         out_relay(2)
 
         offset = (couple * 2 * rows).astype(jnp.float32)
@@ -1129,40 +1155,24 @@
         entering = tuple(jnp.exp(lone + offset * decay_ref[h]) * state_buf[h] for h in range(hr))
         entering = lax.fori_loop(0, couple, gather, entering)
         second = tuple(jnp.exp(lone + float(rows) * decay_ref[h]) * entering[h] + early[h] for h in range(hr))
-
-        def block(i, _):
-            b = jnp.where(i == 0, other, mine)
+        since = lax.broadcasted_iota(jnp.int32, (rows, vd), 0).astype(jnp.float32) + 1.0
+
+        for b in range(2):
             for h in range(hr):
                 rq = part(b, rq_at + h * dk, dk)
-                rk = part(b, rq_at + (hr + h) * dk, dk)
-                rv = part(b, rv_at + h * vd, vd)
-                scores = lax.dot_general(rq, rk, NT, preferred_element_type=jnp.float32) * key_scale
-                scores = jnp.where(causal, scores * jnp.exp(distance * decay_ref[h]), 0.0)
-                inner = jnp.dot(
-                    scores, rv.astype(jnp.float32), precision=highest, preferred_element_type=jnp.float32
-                )
-                leading = jnp.exp((position + 1.0) * decay_ref[h])
                 carried = jnp.dot(
-                    rq.astype(jnp.float32),
-                    jnp.where(b == 0, entering[h], second[h]),
-                    precision=highest,
+                    jnp.concatenate((rq, rq, rq), axis=1),
+                    split((entering, second)[b][h], 0),
                     preferred_element_type=jnp.float32,
                 )
-                raw = inner + carried * leading
+                raw = raw_buf[b, h] + carried * jnp.exp(since * decay_ref[h])
                 center = raw - jnp.mean(raw, axis=-1, keepdims=True)
                 variance = jnp.mean(center * center, axis=-1, keepdims=True)
                 cols = slice(h * vd, (h + 1) * vd)
                 mix_pair[b, :, cols] = (center * lax.rsqrt(variance + epsilon) * hgain_buf[:, cols]).astype(
                     jnp.bfloat16
                 )
-
-            @pl.when(i == 0)
-            def _():
-                mix_copy(0).start()
-
-            return 0
-
-        lax.fori_loop(0, 2, block, 0)
+        mix_copy(0).start()
         mix_own(0)
         for k in range(3, n):
             out_relay(k)
@@ -1305,6 +1315,8 @@
             pltpu.VMEM((1, hr * vd), f32),
             pltpu.VMEM((fh, n * rows), f32),
             pltpu.VMEM((fh, 2 * rows, lanes), f32),
+            pltpu.VMEM((hr, rows, rows), f32),
+            pltpu.VMEM((2, hr, rows, vd), f32),
             pltpu.VMEM((2, n_tp, rows, feats), bf16),
             pltpu.VMEM((shard, 2 * hr * dk), bf16),
             pltpu.VMEM((n * shard, wide), bf16),

time: 48.3 us -> 46.4 us (0.961)
  Pallas kernels: 47.3 us -> 45.5 us
    pallas_call x1, Pallas kernels: 47.3 us -> 45.5 us  [paired(): pl.pallas_call(functools.partial(pair_kernel, size), out_shape=(pltpu.VME...]
where the time goes in v4:
time: 46.4 us; the launch traced here: 46.2 us
  Pallas kernels  45.5 us (98%)
  other arithmetic  0.75 us (2%)
    pallas_call x1, Pallas kernels, paired(): pl.pallas_call(functools.partial(pair_kernel, size), out_shape=(pltpu.VME...  45.5 us

profile of v4, /device:TPU:17, one launch (start us, length us, event | category | flops | bytes accessed | tf_op | source)
XLA Modules:
  0.0 46.2 jit_solution(517230645430046320)
XLA Ops:
  0.0 45.5 %layer.1 = (f32[64,2048]{1,0:T(8,128)S(1)}, bf16[1,64,2048]{2,1,0:T(8,128)(2,1)S(1)}) custom-call(bf16[256,512]{1,0:T(8,128)(2,1)} %tok_ref.1, f32[1,2048]{1,0:T(1,128)} %bitcast.10, bf16[64,512]{1,0:T(8,128)(2,1)} %bitcast.8, bf16[64,512]{1,0:T(8,128)(2,1)} %bitcast.9, bf16[512,128]{1,0:T(8,128)(2,1)} %wrv_ref.1, bf16[512,128]{1,0:T(8,128)(2,1)} %wfq_ref.1, ...), custom_call_target="tpu_custom_call" | custom-call | tf_op jit(solution)/shard_map/layer/pallas_call | solution.py:1306
  45.5 0.8 %fusion = bf16[64,2048]{1,0:T(8,128)(2,1)} fusion(f32[64,2048]{1,0:T(8,128)S(1)} %get-tuple-element.7, bf16[1,64,2048]{2,1,0:T(8,128)(2,1)S(1)} %get-tuple-element.8), kind=kLoop, calls=%fused_computation.1 | loop fusion | flops 393216 | bytes 1048576 | tf_op jit(solution)/shard_map/convert_element_type | solution.py:1387

commit v5 on v4

--- a/solution.py
+++ b/solution.py
@@ -537,6 +537,7 @@
     gate_buf,
     within_buf,
     raw_buf,
+    sums_buf,
     tok_buf,
     qk_own,
     w_buf,
@@ -731,6 +732,7 @@
         start = pl.multiple_of(src * shard + part * step, step)
         return w_buf.at[pl.ds(start, step), starts[c][0] : starts[c][1]]
 
+    far = list(range(2, n - 1))
     local_at = {c: c - group[0] for group in (fox_arrays, ret_arrays) for c in group}
 
     def w_recv(c, src):
@@ -748,9 +750,22 @@
         here = w_at(c, src, g)
         return rdma(here, here, w_s.at[c], w_recv(c, src), sp=src)
 
-    def w_side(c, src, d):
-        here = w_at(c, src, g)
-        return rdma(here, here, wy_s.at[local_at[c]], wy_r.at[local_at[c]], grp=lax.rem(g + d, n_grp))
+    def w_side(c, k, d):
+        here = w_at(c, toward(k), g)
+        return rdma(here, here, wy_s.at[local_at[c]], wy_r.at[wy_at(c, k in late_of(c))], grp=lax.rem(g + d, n_grp))
+
+    def late_of(c):
+        return far if c in fox_arrays else [n - 1]
+
+    def wy_at(c, late):
+        return local_at[c] + (len(fox_arrays) if late and c not in (0, 1) else 0)
+
+    def w_late(c):
+        drained(wy_r.at[wy_at(c, True)], w_several(c, len(late_of(c)) * (n_grp - 1)))
+
+    def w_early(c):
+        w_local(c).wait()
+        drained(wy_r.at[wy_at(c, False)], w_several(c, (n - 1 - len(late_of(c))) * (n_grp - 1)))
 
     def w_several(c, pieces):
         return w_buf.at[: pieces * step, starts[c][0] : starts[c][1]]
@@ -787,16 +802,22 @@
         passes = ((p if up < n else 0) + (n - 1 - p if down >= 0 else 0)) if uses else 0
         return (up < n) + (down >= 0) + passes
 
+    def swap_tokens():
+        for m in range(chunks):
+            tok_z(m).start()
+
     send_weights((0, 1))
     for m in range(chunks):
-        tok_z(m).start()
         tok_c(True, m, 0).start()
-    send_weights((2,))
+
+    swap_tokens()
     meet_far()
     send_weights((3,))
     drained(in_sem.at[0], wqk_buf)
     qk_own[...] = wqk_buf[...].astype(jnp.float32).T.astype(jnp.bfloat16)
     send_weights((4,))
+
+    send_weights((2,))
     tok_local.start()
 
     @pl.when(is_fox)
@@ -806,7 +827,8 @@
 
     @pl.when(is_ret)
     def _():
-        w_local(3).start()
+        for c in ret_arrays:
+            w_local(c).start()
 
     depth = mix_buf.shape[1] // 2
     out_cols = ret_out_ref.shape[1]
@@ -882,7 +904,7 @@
                 w_in(c, toward(i)).wait_recv()
                 w_pass(c, toward(i))
                 for d in range(1, n_grp):
-                    w_side(c, toward(i), d).start()
+                    w_side(c, i, d).start()
 
     def w_arrive(arrays):
         for c in arrays:
@@ -901,7 +923,6 @@
             cols = slice(i * feats, (i + 1) * feats)
             norm_buf[at, cols] = (part * scale * gain_buf[:, cols]).astype(jnp.bfloat16)
 
-    far = list(range(2, n - 1))
 
     def tok_own():
         for d in range(1, half):
@@ -932,22 +953,24 @@
     def _():
         w_relay((0, 1), [1, n - 1])
 
-    @pl.when(is_ret)
-    def _():
-        w_local(4).start()
-
-    tok_swap(0)
-    tok_own()
-    for m in range(1, chunks):
-        tok_swap(m)
-
     @pl.when(is_fox)
     def _():
+        tok_swap(0)
+        tok_own()
+        for m in range(1, chunks):
+            tok_swap(m)
         w_relay((0, 1), far)
         w_relay((2,), [1, n - 1])
 
     @pl.when(is_ret)
     def _():
+        tok_own()
+        for m in range(chunks):
+            tok_swap(m)
+            if m == 1:
+                w_relay((3,), far)
+            if m == 2:
+                w_relay((4,), far)
         w_relay(ret_arrays, [1])
 
     out_begin()
@@ -1005,31 +1028,40 @@
             ).astype(jnp.bfloat16)
             later(lambda q: kv_copy(b, q).start())
 
+        def q_part(srcs):
+            total = 0.0
+            for src in srcs:
+                cols = pl.ds(pl.multiple_of(src * shard, shard), shard)
+                total = total + jnp.dot(
+                    norm_buf[:, cols], w_buf[cols, q_at:fox_wide], preferred_element_type=jnp.float32
+                )
+            return total
+
+        for b in range(2):
+            for h in range(fh):
+                own_cols = pl.ds(pl.multiple_of((2 * couple + b) * rows, rows), rows)
+                own = jnp.where(row_id == col_id, gates_buf[h : h + 1, own_cols], 0.0)
+                gate_buf[h, b * rows : (b + 1) * rows] = jnp.broadcast_to(
+                    jnp.sum(own, axis=1, keepdims=True), (rows, lanes)
+                )
         after_tokens()
         w_arrive((0, 1))
         project_kv(mine)
+        w_relay((2,), far)
+        out_relay(1)
         tok_ready(False)
         normalize(other)
         project_kv(other)
-        w_relay((2,), far)
-        out_relay(1)
-        w_arrive((2,))
-        proj_buf[:, : fh * fd] = jnp.dot(
-            norm_buf[...], w_buf[:, q_at:fox_wide], preferred_element_type=jnp.float32
-        ).astype(jnp.bfloat16)
+        w_early(2)
+        sums_buf[:, : fh * fd] = q_part([me, toward(1), toward(n - 1)])
+        w_late(2)
+        proj_buf[:, : fh * fd] = (sums_buf[:, : fh * fd] + q_part([toward(k) for k in far])).astype(jnp.bfloat16)
 
         def block_cols(at):
             return pl.ds(pl.multiple_of(at * rows, rows), rows)
 
         def rep_cols(x, wide):
             return jnp.concatenate([x] * (wide // lanes), axis=1)
-
-        for b in range(2):
-            for h in range(fh):
-                own = jnp.where(row_id == col_id, gates_buf[h : h + 1, block_cols(2 * couple + b)], 0.0)
-                gate_buf[h, b * rows : (b + 1) * rows] = jnp.broadcast_to(
-                    jnp.sum(own, axis=1, keepdims=True), (rows, lanes)
-                )
 
         def attend(at, top_row, first, offset):
             size_ = 2 * rows - top_row
@@ -1061,6 +1093,7 @@
 
         attend(2 * couple, 0, True, 0)
         attend(2 * couple + 1, rows, False, 0)
+        out_relay(2)
 
         def past(i, _):
             q = lax.div(i, 2)
@@ -1079,7 +1112,7 @@
                 ).astype(jnp.bfloat16)
         mix_copy(depth).start()
         mix_own(depth)
-        for k in range(2, n):
+        for k in range(3, n):
             out_relay(k)
         mix_in(0).wait_recv()
         mix_copy(depth).wait_send()
@@ -1092,16 +1125,27 @@
         key_scale = dk ** (-0.5)
         for h in range(hr):
             within_buf[h] = jnp.where(causal, jnp.exp(distance * decay_ref[h]) * key_scale, 0.0)
+        w_relay(ret_arrays, [n - 1])
         after_tokens()
-        w_relay(ret_arrays, far)
         tok_ready(False)
         normalize(other)
-        w_relay(ret_arrays, [n - 1])
         out_relay(1)
-        w_arrive(ret_arrays)
-        proj_buf[:, :ret_wide] = jnp.dot(
-            norm_buf[...], w_buf[:, :ret_wide], preferred_element_type=jnp.float32
-        ).astype(jnp.bfloat16)
+
+        def ret_part(srcs):
+            total = 0.0
+            for src in srcs:
+                cols = pl.ds(pl.multiple_of(src * shard, shard), shard)
+                total = total + jnp.dot(
+                    norm_buf[:, cols], w_buf[cols, :ret_wide], preferred_element_type=jnp.float32
+                )
+            return total
+
+        for c in ret_arrays:
+            w_early(c)
+        sums_buf[:, :ret_wide] = ret_part([me] + [toward(k) for k in range(1, n - 1)])
+        for c in ret_arrays:
+            w_late(c)
+        proj_buf[:, :ret_wide] = (sums_buf[:, :ret_wide] + ret_part([toward(n - 1)])).astype(jnp.bfloat16)
         rv_at, rq_at = starts[3][0], starts[4][0]
         lone = jnp.zeros((dk, vd), jnp.float32)
 
@@ -1317,6 +1361,7 @@
             pltpu.VMEM((fh, 2 * rows, lanes), f32),
             pltpu.VMEM((hr, rows, rows), f32),
             pltpu.VMEM((2, hr, rows, vd), f32),
+            pltpu.VMEM((2 * rows, wide), f32),
             pltpu.VMEM((2, n_tp, rows, feats), bf16),
             pltpu.VMEM((shard, 2 * hr * dk), bf16),
             pltpu.VMEM((n * shard, wide), bf16),
@@ -1344,7 +1389,7 @@
             dma((5,)),
             dma((3 * n,)),
             dma((3,)),
-            dma((3,)),
+            dma((6,)),
             dma((3,)),
             dma,
             dma((n,)),

time: 46.4 us -> 44.4 us (0.957)
  the two profiles are of different devices: /device:TPU:17 before, /device:TPU:25 now
where the time goes in v5:
time: 44.4 us; the launch traced here: 44.1 us
  Pallas kernels  43.3 us (98%)
  other arithmetic  0.75 us (2%)
    pallas_call x1, Pallas kernels, paired(): pl.pallas_call(functools.partial(pair_kernel, size), out_shape=(pltpu.VME...  43.3 us

profile of v5, /device:TPU:25, one launch (start us, length us, event | category | flops | bytes accessed | tf_op | source)
XLA Modules:
  0.0 44.1 jit_solution(8447748977416227408)
XLA Ops:
  0.0 43.3 %layer.1 = (f32[64,2048]{1,0:T(8,128)S(1)}, bf16[1,64,2048]{2,1,0:T(8,128)(2,1)S(1)}) custom-call(bf16[256,512]{1,0:T(8,128)(2,1)} %tok_ref.1, f32[1,2048]{1,0:T(1,128)} %bitcast.10, bf16[64,512]{1,0:T(8,128)(2,1)} %bitcast.8, bf16[64,512]{1,0:T(8,128)(2,1)} %bitcast.9, bf16[512,128]{1,0:T(8,128)(2,1)} %wrv_ref.1, bf16[512,128]{1,0:T(8,128)(2,1)} %wfq_ref.1, ...), custom_call_target="tpu_custom_call" | custom-call | tf_op jit(solution)/shard_map/layer/pallas_call | solution.py:1350
  43.3 0.8 %fusion = bf16[64,2048]{1,0:T(8,128)(2,1)} fusion(f32[64,2048]{1,0:T(8,128)S(1)} %get-tuple-element.7, bf16[1,64,2048]{2,1,0:T(8,128)(2,1)S(1)} %get-tuple-element.8), kind=kLoop, calls=%fused_computation.1 | loop fusion | flops 393216 | bytes 1048576 | tf_op jit(solution)/shard_map/convert_element_type | solution.py:1432

commit v6 on v5

--- a/solution.py
+++ b/solution.py
@@ -521,7 +521,7 @@
     wfq_ref,
     wfk_ref,
     wfv_ref,
-    decay_ref,
+    decay_hbm,
     state_ref,
     hgain_ref,
     gates_ref,
@@ -529,6 +529,7 @@
     fox_out_ref,
     near_ref,
     far_ref,
+    decay_ref,
     gain_buf,
     wqk_buf,
     state_buf,
@@ -636,7 +637,7 @@
     brought = [
         pltpu.make_async_copy(src, dst, in_sem.at[i + 1])
         for i, (src, dst) in enumerate(
-            ((gain_ref, gain_buf), (state_ref, state_buf), (hgain_ref, hgain_buf), (gates_ref, gates_buf))
+            ((gain_ref, gain_buf), (state_ref, state_buf), (hgain_ref, hgain_buf), (gates_ref, gates_buf), (decay_hbm, decay_ref))
         )
     ]
     for copy in brought:
@@ -782,15 +783,15 @@
     ret_down = jnp.where(is_fox & (mine == 1), partner, jnp.where(couple >= 1, ret_of(jnp.maximum(couple - 1, 0)), -1))
 
     def send_weights(arrays):
-        up, down = (fox_up, fox_down) if arrays[0] in fox_arrays else (ret_up, ret_down)
         for c in arrays:
+            up, down = (fox_up, fox_down) if c in fox_arrays else (ret_up, ret_down)
 
             @pl.when(up < n)
-            def _(c=c):
+            def _(c=c, up=up):
                 w_send(c, up).start()
 
             @pl.when(down >= 0)
-            def _(c=c):
+            def _(c=c, down=down):
                 w_send(c, down).start()
 
     def sends_from(p, arrays):
@@ -811,13 +812,20 @@
         tok_c(True, m, 0).start()
 
     swap_tokens()
+
+    @pl.when(is_ret)
+    def _():
+        send_weights((2,))
+
     meet_far()
     send_weights((3,))
     drained(in_sem.at[0], wqk_buf)
     qk_own[...] = wqk_buf[...].astype(jnp.float32).T.astype(jnp.bfloat16)
-    send_weights((4,))
-
-    send_weights((2,))
+
+    @pl.when(is_ret)
+    def _():
+        send_weights((4,))
+
     tok_local.start()
 
     @pl.when(is_fox)
@@ -847,7 +855,7 @@
 
     def out_hop(c, src, to, first):
         here = out_refs[c].at[pl.ds(pl.multiple_of(g * out_step, out_step), out_step)] if first else out_at(c, src)
-        return rdma(here, out_at(c, src), o_s, o_r.at[src], sp=to)
+        return rdma(here, out_at(c, src), o_s, o_r.at[2 * src + c], sp=to)
 
     def out_local(c):
         return pltpu.make_async_copy(out_refs[c], wout_buf.at[c * depth : (c + 1) * depth, out_cols_of(me)], o_loc)
@@ -870,9 +878,9 @@
 
             @pl.when((src >= 0) & (src < n))
             def _(src=src, to=to):
-                both = out_both(src)
-                rdma(both, both, o_s, o_r.at[src], sp=src).wait_recv()
                 for c in range(2):
+                    there = out_at(c, src)
+                    rdma(there, there, o_s, o_r.at[2 * src + c], sp=src).wait_recv()
 
                     @pl.when((to >= 0) & (to < n))
                     def _(c=c):
@@ -952,6 +960,7 @@
     @pl.when(is_fox)
     def _():
         w_relay((0, 1), [1, n - 1])
+        send_weights((4, 2))
 
     @pl.when(is_fox)
     def _():
@@ -984,17 +993,28 @@
     def norm_rows(h):
         return norm_buf[pl.ds(pl.multiple_of(h * rows, rows), rows), :]
 
-    def mix_copy(first):
-        return rdma(
-            mix_pair.at[other], mix_buf.at[:, first : first + depth], mix_s, mix_r, sp=partner
-        )
+    block = rows // n_tp
+    span = 2 * block
+
+    def mix_rows(d):
+        return pl.ds(pl.multiple_of(lax.rem(pair + d, half) * span, span), span)
+
+    away = [*range(1, half), 0]
+
+    def mix_copy(first, d):
+        here = mix_pair.at[other, mix_rows(d)]
+        return rdma(here, mix_buf.at[mix_rows(d), first : first + depth], mix_s.at[d], mix_r.at[d], sp=partner)
+
+    def mix_send(first):
+        for d in away:
+            mix_copy(first, d).start()
 
     def mix_own(first):
         mix_buf[:, first : first + depth] = mix_pair[mine]
 
-    def mix_in(first):
-        here = mix_buf.at[:, first : first + depth]
-        return rdma(here, here, mix_s, mix_r, sp=partner)
+    def mix_in(d):
+        here = mix_buf.at[mix_rows(d), :depth]
+        rdma(here, here, mix_s.at[d], mix_r.at[d], sp=partner).wait_recv()
 
     def kv_copy(b, q):
         at = 2 * couple + b
@@ -1110,12 +1130,12 @@
                 mix_pair[b, :, h * fd : (h + 1) * fd] = (
                     weighted_buf[h, at] / total_buf[h, at, :fd]
                 ).astype(jnp.bfloat16)
-        mix_copy(depth).start()
+        mix_send(depth)
         mix_own(depth)
         for k in range(3, n):
             out_relay(k)
-        mix_in(0).wait_recv()
-        mix_copy(depth).wait_send()
+        for d in away:
+            mix_copy(depth, d).wait_send()
         later(lambda q: kv_copy(0, q).wait_send())
         later(lambda q: kv_copy(1, q).wait_send())
 
@@ -1216,59 +1236,59 @@
                 mix_pair[b, :, cols] = (center * lax.rsqrt(variance + epsilon) * hgain_buf[:, cols]).astype(
                     jnp.bfloat16
                 )
-        mix_copy(0).start()
+        mix_send(0)
         mix_own(0)
         for k in range(3, n):
             out_relay(k)
-        mix_in(depth).wait_recv()
-        mix_copy(0).wait_send()
+        for d in away:
+            mix_copy(0, d).wait_send()
         later(lambda q: sum_copy(q).wait_send())
 
-    block = rows // n_tp
     wide, pieces = out_cols, n
 
     def piece_cols(piece):
         return pl.ds(pl.multiple_of(piece * wide, wide), wide)
 
-    def slot(at):
-        return pl.ds(pl.multiple_of(at * block, block), block)
-
-    def pair_copy(piece):
+    def slot(d):
+        return pl.ds(pl.multiple_of(lax.rem(pair + d, half) * block, block), block)
+
+    def pair_copy(piece, d):
         cols = piece_cols(piece)
         return rdma(
-            rs_send.at[1 - parity, :, cols],
-            pair_buf.at[:, cols],
+            rs_send.at[1 - parity, slot(d), cols],
+            pair_buf.at[slot(d), cols],
             pair_s,
-            pair_r.at[piece],
+            pair_r.at[piece * half + d],
             tp=t + 1 - 2 * parity,
         )
 
     def rs_copy(d, piece):
-        to = lax.rem(pair + d, half)
         cols = piece_cols(piece)
         return rdma(
-            pair_sum.at[slot(to), cols],
+            pair_sum.at[slot(d), cols],
             far_ref.at[d - 1, :, cols],
             rs_s.at[d - 1],
             rs_r.at[d - 1],
-            tp=2 * to + parity,
+            tp=2 * lax.rem(pair + d, half) + parity,
         )
 
-    def project(piece):
+    def project(piece, d):
         cols = piece_cols(piece)
-        value = jnp.dot(mix_buf[...], wout_buf[:, cols], preferred_element_type=jnp.float32).astype(jnp.bfloat16)
-        for b in range(n_tp):
-            at = slice(b // 2 * block, (b // 2 + 1) * block)
-            rs_send[b % 2, at, cols] = value[b * block : (b + 1) * block]
-        pair_copy(piece).start()
-
-    def reduce(piece):
+        value = jnp.dot(mix_buf[mix_rows(d), :], wout_buf[:, cols], preferred_element_type=jnp.float32)
+        value = value.astype(jnp.bfloat16)
+        for b in range(2):
+            rs_send[b, slot(d), cols] = value[b * block : (b + 1) * block]
+        pair_copy(piece, d).start()
+
+    def reduce(piece, d):
         cols = piece_cols(piece)
-        pair_copy(piece).wait_recv()
-        both = rs_send[parity, :, cols].astype(jnp.float32) + pair_buf[:, cols].astype(jnp.float32)
-        pair_sum[:, cols] = both.astype(jnp.bfloat16)
-        for d in range(1, half):
+        pair_copy(piece, d).wait_recv()
+        both = rs_send[parity, slot(d), cols].astype(jnp.float32) + pair_buf[slot(d), cols].astype(jnp.float32)
+        if d:
+            pair_sum[slot(d), cols] = both.astype(jnp.bfloat16)
             rs_copy(d, piece).start()
+        else:
+            near_ref[:, cols] = both
 
     def order(i):
         falling = jnp.where(i <= me, me - i, i)
@@ -1276,19 +1296,25 @@
         return jnp.where(lower, rising, falling)
 
     drained(o_loc, wout_buf.at[:, out_cols_of(me)])
-    project(me)
+    for d in range(1, half):
+        mix_in(d)
+        project(me, d)
+    mix_in(0)
 
     def turn(i, _):
         out_arrive(order(i))
-        project(order(i))
-        reduce(order(i - 1))
+        for d in range(1, half):
+            project(order(i), d)
+            reduce(order(i - 1), d)
+        project(order(i - 1), 0)
         return 0
 
     lax.fori_loop(1, n, turn, 0)
-    reduce(order(jnp.int32(n - 1)))
-
-    own = slot(pair)
-    near_ref[...] = rs_send[parity, own, :].astype(jnp.float32) + pair_buf[own, :].astype(jnp.float32)
+    for d in range(1, half):
+        reduce(order(jnp.int32(n - 1)), d)
+    project(order(jnp.int32(n - 1)), 0)
+    for piece in range(pieces):
+        reduce(piece, 0)
 
     slabs = rows * (2 * n_tp - 1) // (2 * n_tp)
     drained(t_s, tok_buf.at[:, :, :slabs])
@@ -1343,16 +1369,16 @@
     far = max(half - 1, 1)
     side = max(n_grp - 1, 1) * n
     vmem = pl.BlockSpec(memory_space=pltpu.VMEM)
-    smem = pl.BlockSpec(memory_space=pltpu.SMEM)
     hbm = pl.BlockSpec(memory_space=pl.ANY)
     bf16, f32 = jnp.bfloat16, jnp.float32
     size = (n, n_tp, n_grp, hr, dk, vd, fh, fd, chunks)
     near, other = pl.pallas_call(
         functools.partial(pair_kernel, size),
         out_shape=(pltpu.VMEM((block, columns), f32), pltpu.VMEM((far, block, columns), bf16)),
-        in_specs=[hbm] * 8 + [smem] + [hbm] * 5,
+        in_specs=[hbm] * 14,
         out_specs=(vmem, vmem),
         scratch_shapes=[
+            pltpu.SMEM((hr,), f32),
             pltpu.VMEM((1, n_tp * feats), f32),
             pltpu.VMEM((2 * hr * dk, shard), bf16),
             pltpu.VMEM((hr, dk, vd), f32),
@@ -1378,7 +1404,7 @@
             pltpu.VMEM((fh, 2 * rows, lanes), f32),
             pltpu.VMEM((fh, 2 * rows, lanes), f32),
             pltpu.VMEM((fh, 2 * rows, fd), f32),
-            dma((5,)),
+            dma((6,)),
             pltpu.SemaphoreType.REGULAR,
             pltpu.SemaphoreType.REGULAR,
             dma,
@@ -1392,7 +1418,7 @@
             dma((6,)),
             dma((3,)),
             dma,
-            dma((n,)),
+            dma((2 * n,)),
             dma,
             dma((side,)),
             dma,
@@ -1400,10 +1426,10 @@
             dma((n,)),
             dma((couples,)),
             dma((couples,)),
+            dma((half,)),
+            dma((half,)),
             dma,
-            dma,
-            dma,
-            dma((n,)),
+            dma((n * half,)),
             dma((far,)),
             dma((far,)),
         ],

time: 44.4 us -> 43.1 us (0.971)
  Pallas kernels: 43.3 us -> 42.2 us
    pallas_call x1, Pallas kernels: 43.3 us -> 42.2 us  [paired(): pl.pallas_call(functools.partial(pair_kernel, size), out_shape=(pltpu.VME...]
where the time goes in v6:
time: 43.1 us; the launch traced here: 43 us
  Pallas kernels  42.2 us (98%)
  other arithmetic  0.75 us (2%)
    pallas_call x1, Pallas kernels, paired(): pl.pallas_call(functools.partial(pair_kernel, size), out_shape=(pltpu.VME...  42.2 us

profile of v6, /device:TPU:25, one launch (start us, length us, event | category | flops | bytes accessed | tf_op | source)
XLA Modules:
  0.0 43.0 jit_solution(17712511728159994304)
XLA Ops:
  0.0 42.2 %layer.1 = (f32[64,2048]{1,0:T(8,128)S(1)}, bf16[1,64,2048]{2,1,0:T(8,128)(2,1)S(1)}) custom-call(bf16[256,512]{1,0:T(8,128)(2,1)} %tok_ref.1, f32[1,2048]{1,0:T(1,128)} %bitcast.10, bf16[64,512]{1,0:T(8,128)(2,1)} %bitcast.8, bf16[64,512]{1,0:T(8,128)(2,1)} %bitcast.9, bf16[512,128]{1,0:T(8,128)(2,1)} %wrv_ref.1, bf16[512,128]{1,0:T(8,128)(2,1)} %wfq_ref.1, ...), custom_call_target="tpu_custom_call" | custom-call | tf_op jit(solution)/shard_map/layer/pallas_call | solution.py:1375
  42.2 0.8 %fusion = bf16[64,2048]{1,0:T(8,128)(2,1)} fusion(f32[64,2048]{1,0:T(8,128)S(1)} %get-tuple-element.7, bf16[1,64,2048]{2,1,0:T(8,128)(2,1)S(1)} %get-tuple-element.8), kind=kLoop, calls=%fused_computation.1 | loop fusion | flops 393216 | bytes 1048576 | tf_op jit(solution)/shard_map/convert_element_type | solution.py:1458

commit v7 on v6

--- a/solution.py
+++ b/solution.py
@@ -552,6 +552,7 @@
     rs_send,
     pair_buf,
     pair_sum,
+    p_buf,
     top_buf,
     total_buf,
     weighted_buf,
@@ -970,6 +971,7 @@
             tok_swap(m)
         w_relay((0, 1), far)
         w_relay((2,), [1, n - 1])
+        out_begin()
 
     @pl.when(is_ret)
     def _():
@@ -980,9 +982,9 @@
                 w_relay((3,), far)
             if m == 2:
                 w_relay((4,), far)
+        out_begin()
         w_relay(ret_arrays, [1])
 
-    out_begin()
     tok_ready(True)
     normalize(mine)
 
@@ -1016,12 +1018,18 @@
         here = mix_buf.at[mix_rows(d), :depth]
         rdma(here, here, mix_s.at[d], mix_r.at[d], sp=partner).wait_recv()
 
-    def kv_copy(b, q):
-        at = 2 * couple + b
-        return rdma(kv_buf.at[at], kv_buf.at[at], kv_s.at[2 * q + b], kv_r.at[at], sp=fox_of(q))
-
-    def kv_in(at):
-        return rdma(kv_buf.at[at], kv_buf.at[at], kv_s.at[at], kv_r.at[at], sp=partner)
+    def kv_part(at, values):
+        first = fh * fd if values else 0
+        return kv_buf.at[at, :, first : first + fh * fd]
+
+    def kv_copy(b, q, values):
+        here = kv_part(2 * couple + b, values)
+        send = kv_s.at[2 * (2 * (q - 1) + b) + values]
+        return rdma(here, here, send, kv_r.at[2 * (2 * couple + b) + values], sp=fox_of(q))
+
+    def kv_in(at, values):
+        here = kv_part(at, values)
+        return rdma(here, here, kv_s.at[values], kv_r.at[2 * at + values], sp=partner)
 
     def sum_copy(q):
         return rdma(sum_buf.at[couple], sum_buf.at[couple], sum_s.at[q], sum_r.at[couple], sp=ret_of(q))
@@ -1046,7 +1054,8 @@
             kv_buf[2 * couple + b] = jnp.dot(
                 norm_rows(b), w_buf[:, :q_at], preferred_element_type=jnp.float32
             ).astype(jnp.bfloat16)
-            later(lambda q: kv_copy(b, q).start())
+            for values in range(2):
+                later(lambda q, values=values: kv_copy(b, q, values).start())
 
         def q_part(srcs):
             total = 0.0
@@ -1119,8 +1128,29 @@
             q = lax.div(i, 2)
             b = jnp.where(lax.rem(i, 2) == 0, fox_of(q) - 2 * q, 1 - (fox_of(q) - 2 * q))
             at = 2 * q + b
-            kv_in(at).wait_recv()
-            attend(at, 0, False, None)
+            kv_in(at, 0).wait_recv()
+            for h in range(fh):
+                k = kv_buf[at, :, h * fd : (h + 1) * fd]
+                logits = lax.dot_general(
+                    proj_buf[:, h * fd : (h + 1) * fd], k, NT, preferred_element_type=jnp.float32
+                ) * fd ** (-0.5)
+                logits = logits + rep_cols(gate_buf[h], rows) - gates_buf[h : h + 1, block_cols(at)]
+                top = top_buf[h]
+                top_new = jnp.maximum(
+                    top, jnp.broadcast_to(jnp.max(logits, axis=-1, keepdims=True), (2 * rows, lanes))
+                )
+                p = jnp.exp(logits - rep_cols(top_new, rows))
+                rescale = jnp.exp(top - top_new)
+                top_buf[h] = top_new
+                total_buf[h] = total_buf[h] * rescale + jnp.broadcast_to(
+                    jnp.sum(p, axis=-1, keepdims=True), (2 * rows, lanes)
+                )
+                weighted_buf[h] = weighted_buf[h] * rescale[:, :fd]
+                p_buf[h] = p.astype(jnp.bfloat16)
+            kv_in(at, 1).wait_recv()
+            for h in range(fh):
+                v = kv_buf[at, :, (fh + h) * fd : (fh + h + 1) * fd]
+                weighted_buf[h] = weighted_buf[h] + jnp.dot(p_buf[h], v, preferred_element_type=jnp.float32)
             return 0
 
         lax.fori_loop(0, 2 * couple, past, 0)
@@ -1134,10 +1164,6 @@
         mix_own(depth)
         for k in range(3, n):
             out_relay(k)
-        for d in away:
-            mix_copy(depth, d).wait_send()
-        later(lambda q: kv_copy(0, q).wait_send())
-        later(lambda q: kv_copy(1, q).wait_send())
 
     @pl.when(is_ret)
     def _():
@@ -1240,9 +1266,6 @@
         mix_own(0)
         for k in range(3, n):
             out_relay(k)
-        for d in away:
-            mix_copy(0, d).wait_send()
-        later(lambda q: sum_copy(q).wait_send())
 
     wide, pieces = out_cols, n
 
@@ -1338,10 +1361,18 @@
     @pl.when(is_fox)
     def _():
         sides(fox_arrays)
+        for d in away:
+            mix_copy(depth, d).wait_send()
+        for b in range(2):
+            for values in range(2):
+                later(lambda q, b=b, values=values: kv_copy(b, q, values).wait_send())
 
     @pl.when(is_ret)
     def _():
         sides(ret_arrays)
+        for d in away:
+            mix_copy(0, d).wait_send()
+        later(lambda q: sum_copy(q).wait_send())
 
     drained(pair_s, pair_buf)
     for d in range(1, half):
@@ -1401,6 +1432,7 @@
             pltpu.VMEM((2, rows // 2, columns), bf16),
             pltpu.VMEM((rows // 2, columns), bf16),
             pltpu.VMEM((rows // 2, columns), bf16),
+            pltpu.VMEM((fh, 2 * rows, rows), bf16),
             pltpu.VMEM((fh, 2 * rows, lanes), f32),
             pltpu.VMEM((fh, 2 * rows, lanes), f32),
             pltpu.VMEM((fh, 2 * rows, fd), f32),
@@ -1422,8 +1454,8 @@
             dma,
             dma((side,)),
             dma,
-            dma((2 * couples,)),
-            dma((n,)),
+            dma((4 * (couples - 1),)),
+            dma((2 * (n - 2),)),
             dma((couples,)),
             dma((couples,)),
             dma((half,)),

time: 43.1 us -> 42.5 us (0.986)
  Pallas kernels: 42.2 us -> 41.6 us
    pallas_call x1, Pallas kernels: 42.2 us -> 41.6 us  [paired(): pl.pallas_call(functools.partial(pair_kernel, size), out_shape=(pltpu.VME...]
where the time goes in v7:
time: 42.5 us; the launch traced here: 42.4 us
  Pallas kernels  41.6 us (98%)
  other arithmetic  0.75 us (2%)
    pallas_call x1, Pallas kernels, paired(): pl.pallas_call(functools.partial(pair_kernel, size), out_shape=(pltpu.VME...  41.6 us

profile of v7, /device:TPU:25, one launch (start us, length us, event | category | flops | bytes accessed | tf_op | source)
XLA Modules:
  0.0 42.4 jit_solution(14171592839354271204)
XLA Ops:
  0.0 41.6 %layer.1 = (f32[64,2048]{1,0:T(8,128)S(1)}, bf16[1,64,2048]{2,1,0:T(8,128)(2,1)S(1)}) custom-call(bf16[256,512]{1,0:T(8,128)(2,1)} %tok_ref.1, f32[1,2048]{1,0:T(1,128)} %bitcast.10, bf16[64,512]{1,0:T(8,128)(2,1)} %bitcast.8, bf16[64,512]{1,0:T(8,128)(2,1)} %bitcast.9, bf16[512,128]{1,0:T(8,128)(2,1)} %wrv_ref.1, bf16[512,128]{1,0:T(8,128)(2,1)} %wfq_ref.1, ...), custom_call_target="tpu_custom_call" | custom-call | tf_op jit(solution)/shard_map/layer/pallas_call | solution.py:1406
  41.6 0.8 %fusion = bf16[64,2048]{1,0:T(8,128)(2,1)} fusion(f32[64,2048]{1,0:T(8,128)S(1)} %get-tuple-element.7, bf16[1,64,2048]{2,1,0:T(8,128)(2,1)S(1)} %get-tuple-element.8), kind=kLoop, calls=%fused_computation.1 | loop fusion | flops 393216 | bytes 1048576 | tf_op jit(solution)/shard_map/convert_element_type | solution.py:1490

commit v8 on v7

--- a/solution.py
+++ b/solution.py
@@ -973,8 +973,15 @@
         w_relay((2,), [1, n - 1])
         out_begin()
 
+    row_id = lax.broadcasted_iota(jnp.int32, (rows, rows), 0)
+    col_id = lax.broadcasted_iota(jnp.int32, (rows, rows), 1)
+
     @pl.when(is_ret)
     def _():
+        distance = jnp.maximum(row_id - col_id, 0).astype(jnp.float32)
+        for h in range(hr):
+            within = jnp.exp(distance * decay_ref[h]) * dk ** (-0.5)
+            within_buf[h] = jnp.where(col_id <= row_id, within, 0.0)
         tok_own()
         for m in range(chunks):
             tok_swap(m)
@@ -987,10 +994,6 @@
 
     tok_ready(True)
     normalize(mine)
-
-    row_id = lax.broadcasted_iota(jnp.int32, (rows, rows), 0)
-    col_id = lax.broadcasted_iota(jnp.int32, (rows, rows), 1)
-    causal = col_id <= row_id
 
     def norm_rows(h):
         return norm_buf[pl.ds(pl.multiple_of(h * rows, rows), rows), :]
@@ -1167,10 +1170,7 @@
 
     @pl.when(is_ret)
     def _():
-        distance = jnp.maximum(row_id - col_id, 0).astype(jnp.float32)
         key_scale = dk ** (-0.5)
-        for h in range(hr):
-            within_buf[h] = jnp.where(causal, jnp.exp(distance * decay_ref[h]) * key_scale, 0.0)
         w_relay(ret_arrays, [n - 1])
         after_tokens()
         tok_ready(False)
@@ -1281,7 +1281,7 @@
             rs_send.at[1 - parity, slot(d), cols],
             pair_buf.at[slot(d), cols],
             pair_s,
-            pair_r.at[piece * half + d],
+            pair_r.at[pieces * (half - 1) if d == 0 else piece * (half - 1) + d - 1],
             tp=t + 1 - 2 * parity,
         )
 
@@ -1305,7 +1305,8 @@
 
     def reduce(piece, d):
         cols = piece_cols(piece)
-        pair_copy(piece, d).wait_recv()
+        if d:
+            pair_copy(piece, d).wait_recv()
         both = rs_send[parity, slot(d), cols].astype(jnp.float32) + pair_buf[slot(d), cols].astype(jnp.float32)
         if d:
             pair_sum[slot(d), cols] = both.astype(jnp.bfloat16)
@@ -1336,6 +1337,7 @@
     for d in range(1, half):
         reduce(order(jnp.int32(n - 1)), d)
     project(order(jnp.int32(n - 1)), 0)
+    drained(pair_r.at[pieces * (half - 1)], pair_buf.at[slot(0)])
     for piece in range(pieces):
         reduce(piece, 0)
 
@@ -1461,7 +1463,7 @@
             dma((half,)),
             dma((half,)),
             dma,
-            dma((n * half,)),
+            dma((n * (half - 1) + 1,)),
             dma((far,)),
             dma((far,)),
         ],

time: 42.5 us -> 42.5 us (level)
  no operation moved by 1% of the time
where the time goes in v8:
time: 42.5 us; the launch traced here: 42.3 us
  Pallas kernels  41.6 us (98%)
  other arithmetic  0.75 us (2%)
    pallas_call x1, Pallas kernels, paired(): pl.pallas_call(functools.partial(pair_kernel, size), out_shape=(pltpu.VME...  41.6 us

profile of v8, /device:TPU:25, one launch (start us, length us, event | category | flops | bytes accessed | tf_op | source)
XLA Modules:
  0.0 42.3 jit_solution(11150573023139289513)
XLA Ops:
  0.0 41.6 %layer.1 = (f32[64,2048]{1,0:T(8,128)S(1)}, bf16[1,64,2048]{2,1,0:T(8,128)(2,1)S(1)}) custom-call(bf16[256,512]{1,0:T(8,128)(2,1)} %tok_ref.1, f32[1,2048]{1,0:T(1,128)} %bitcast.10, bf16[64,512]{1,0:T(8,128)(2,1)} %bitcast.8, bf16[64,512]{1,0:T(8,128)(2,1)} %bitcast.9, bf16[512,128]{1,0:T(8,128)(2,1)} %wrv_ref.1, bf16[512,128]{1,0:T(8,128)(2,1)} %wfq_ref.1, ...), custom_call_target="tpu_custom_call" | custom-call | tf_op jit(solution)/shard_map/layer/pallas_call | solution.py:1408
  41.6 0.8 %fusion = bf16[64,2048]{1,0:T(8,128)(2,1)} fusion(f32[64,2048]{1,0:T(8,128)S(1)} %get-tuple-element.7, bf16[1,64,2048]{2,1,0:T(8,128)(2,1)S(1)} %get-tuple-element.8), kind=kLoop, calls=%fused_computation.1 | loop fusion | flops 393216 | bytes 1048576 | tf_op jit(solution)/shard_map/convert_element_type | solution.py:1492
